TPU v7x, 32 devices: a whole 2x2x4 slice. The times are simulated.
32 devices in a mesh: sp: 8 (over z, y), tp: 4 (over x, core).
Axes of the slice: x: 2, y: 2, z: 4, core: 2. Of those that a mesh axis runs over, the one named last changes fastest.
Arguments:
- tokens: bfloat16 [2048, 2048], P('sp'), may hold values from -72 to 72
- query_weight: bfloat16 [3, 2048, 1024], P(None, None, 'tp'), may hold values from -0.125 to 0.125
- key_weight: bfloat16 [3, 2048, 1024], P(None, None, 'tp'), may hold values from -0.125 to 0.125
- value_weight: bfloat16 [3, 2048, 1024], P(None, None, 'tp'), may hold values from -0.125 to 0.125
- out_weight: bfloat16 [1024, 2048], P(None, 'tp'), may hold values from -2 to 2
Outputs:
- mixed: bfloat16 [2048, 2048], P('sp', 'tp')
All inputs are finite; a program needn't handle non-finite values.
Results may differ from a plain program's by a relative error of at most 0.012.
Values may be sent and summed in bfloat16 or wider, within the bound.
A program may use at most 64 MiB of HBM per device.

v0:
```python
import functools
import math

import jax
import numpy as np
import jax.numpy as jnp
from jax import lax
from jax.experimental import pallas as pl
from jax.experimental.pallas import tpu as pltpu
from jax.sharding import PartitionSpec as P

HEAD_DIM = 64
SIDE_STEPS = 64
MIDDLE_DILATION = 4
FAR_DILATION = 16
MESH = pl.DeviceIdType.MESH


def shifted(block, axis, distance):
    devices = range(lax.axis_size(axis))
    route = [(i - distance, i) for i in devices if i - distance in devices]
    return lax.ppermute(block, axis, route)


def with_halo(block, sides, width):
    for axis, dim in sides:
        count = lax.axis_size(axis)
        forward = [(i, i + 1) for i in range(count - 1)]
        backward = [(target, source) for source, target in forward]
        low = lax.ppermute(
            lax.slice_in_dim(block, block.shape[dim] - width, None, axis=dim), axis, forward
        )
        high = lax.ppermute(lax.slice_in_dim(block, 0, width, axis=dim), axis, backward)
        block = jnp.concatenate([low, block, high], axis=dim)
    return block


def rotate(projected, offset_pos):
    length, columns = projected.shape
    heads = columns // HEAD_DIM
    half = HEAD_DIM // 2
    positions = (offset_pos + jnp.arange(length)).astype(jnp.float32)
    inverse = 1.0 / 10000.0 ** (jnp.arange(half, dtype=jnp.float32) * 2.0 / HEAD_DIM)
    angles = positions[:, None] * inverse[None, :]
    angles = jnp.concatenate([angles, angles], axis=-1)
    cosine_table = jnp.cos(angles)[:, None, :]
    sine = jnp.sin(angles)[:, None, :]
    shaped = projected.reshape(length, heads, HEAD_DIM)
    turned = jnp.concatenate([-shaped[..., half:], shaped[..., :half]], axis=-1)
    return (shaped * cosine_table + turned * sine).reshape(length, columns)


def banded(queries, key_ext, value_ext, dilation, offset_pos, seq_len):
    length, columns = queries.shape
    heads = columns // HEAD_DIM
    class_len = length // dilation
    block_len = math.gcd(SIDE_STEPS, class_len)
    blocks = class_len // block_len
    extra = 2 * SIDE_STEPS // block_len
    query_blocks = queries.reshape(blocks, block_len, dilation, heads, HEAD_DIM)
    key_blocks = key_ext.reshape(blocks + extra, block_len, dilation, heads, HEAD_DIM)
    value_blocks = value_ext.reshape(blocks + extra, block_len, dilation, heads, HEAD_DIM)
    key_win = jnp.concatenate(
        [key_blocks[shift_idx : shift_idx + blocks] for shift_idx in range(extra + 1)], axis=1
    )
    value_win = jnp.concatenate(
        [value_blocks[shift_idx : shift_idx + blocks] for shift_idx in range(extra + 1)], axis=1
    )
    scores = jnp.einsum(
        "bqrhe,bkrhe->brhqk", query_blocks, key_win, preferred_element_type=jnp.float32
    )
    scores = scores * HEAD_DIM ** (-0.5)
    width_keys = key_win.shape[1]
    relative = jnp.arange(width_keys)[None, :] - jnp.arange(block_len)[:, None]
    within = (relative >= 0) & (relative <= 2 * SIDE_STEPS)
    key_rows = jnp.arange(blocks)[:, None] * block_len + jnp.arange(width_keys)[None, :]
    spots = (
        offset_pos
        - SIDE_STEPS * dilation
        + dilation * key_rows[:, :, None]
        + jnp.arange(dilation)[None, None, :]
    )
    inside = (spots >= 0) & (spots < seq_len)
    allowed = within[None, None, None] & jnp.transpose(inside, (0, 2, 1))[:, :, None, None, :]
    scores = jnp.where(allowed, scores, -1e30)
    row_max = jnp.max(scores, axis=-1, keepdims=True)
    expo = jnp.exp(scores - row_max)
    denom = jnp.sum(expo, axis=-1)
    probs = expo.astype(jnp.bfloat16)
    summed = jnp.einsum("brhqk,bkrhe->bqrhe", probs, value_win, preferred_element_type=jnp.float32)
    group_out = summed / jnp.transpose(denom, (0, 3, 1, 2))[..., None]
    log_sum = row_max[..., 0] + jnp.log(denom)
    log_sum = jnp.transpose(log_sum, (0, 3, 1, 2)).reshape(length, heads)
    return (group_out.reshape(length, columns), log_sum)


def collect(own_block, needed, direction):
    collected = own_block[None]
    while collected.shape[0] < needed + 1:
        stride = collected.shape[0]
        to_send = min(stride, needed + 1 - stride)
        arrived = shifted(collected[:to_send], "sp", direction * stride)
        collected = jnp.concatenate([collected, arrived], axis=0)
    return collected[1:]


def per_device(tokens, query_weight, key_weight, value_weight, out_weight):
    length = tokens.shape[0]
    offset_pos = lax.axis_index("sp") * length
    seq_len = lax.axis_size("sp") * length
    group_dilations = (1, MIDDLE_DILATION, FAR_DILATION)
    query_list = []
    pairs = []
    for group_idx in range(3):
        queries = rotate(
            jnp.dot(tokens, query_weight[group_idx], preferred_element_type=jnp.float32), offset_pos
        )
        keys_here = rotate(
            jnp.dot(tokens, key_weight[group_idx], preferred_element_type=jnp.float32), offset_pos
        )
        values_here = jnp.dot(tokens, value_weight[group_idx], preferred_element_type=jnp.float32)
        query_list.append(queries.astype(jnp.bfloat16))
        pairs.append(
            jnp.stack([keys_here.astype(jnp.bfloat16), values_here.astype(jnp.bfloat16)], axis=0)
        )
    middle_span_length = SIDE_STEPS * MIDDLE_DILATION
    first_ext = with_halo(pairs[0], (("sp", 1),), SIDE_STEPS)
    middle_ext = with_halo(pairs[1], (("sp", 1),), middle_span_length)
    far_span_length = SIDE_STEPS * FAR_DILATION
    needed = -(-far_span_length // length)
    lower_blocks = collect(pairs[2], needed, 1)
    upper_blocks = collect(pairs[2], needed, -1)
    columns = pairs[2].shape[2]
    lower_flat = jnp.moveaxis(lower_blocks[::-1], 0, 1).reshape(2, needed * length, columns)
    upper_flat = jnp.moveaxis(upper_blocks, 0, 1).reshape(2, needed * length, columns)
    far_full = jnp.concatenate([lower_flat, pairs[2], upper_flat], axis=1)
    extended = (first_ext, middle_ext, far_full)
    outputs = []
    log_sums = []
    for group_idx in range(3):
        group_out, log_sum = banded(
            query_list[group_idx],
            extended[group_idx][0],
            extended[group_idx][1],
            group_dilations[group_idx],
            offset_pos,
            seq_len,
        )
        outputs.append(group_out)
        log_sums.append(log_sum)
    merge_w = jax.nn.softmax(jnp.stack(log_sums, axis=0), axis=0)
    heads = columns // HEAD_DIM
    stacked = jnp.stack(outputs, axis=0).reshape(3, length, heads, HEAD_DIM)
    merged = (
        jnp.sum(merge_w[..., None] * stacked, axis=0).reshape(length, columns).astype(jnp.bfloat16)
    )
    mixed = jnp.dot(
        lax.all_gather(merged, "tp", axis=1, tiled=True),
        out_weight,
        preferred_element_type=jnp.float32,
    )
    return mixed.astype(jnp.bfloat16)


def remote(src, dst, send_sem, recv_sem, axis, target):
    return pltpu.make_async_remote_copy(
        src_ref=src,
        dst_ref=dst,
        send_sem=send_sem,
        recv_sem=recv_sem,
        device_id={axis: target},
        device_id_type=MESH,
    )


def head_mask(columns, head):
    lane = lax.broadcasted_iota(jnp.int32, (1, columns), 1)
    return (lane // HEAD_DIM == head).astype(jnp.float32)


def attend(queries, keys, values, bias):
    rows, columns = queries.shape
    heads = columns // HEAD_DIM
    masks = [head_mask(columns, head) for head in range(heads)]
    stacked = jnp.concatenate([queries * mask.astype(jnp.bfloat16) for mask in masks], axis=0)
    scores = lax.dot_general(
        stacked, keys, (((1,), (1,)), ((), ())), preferred_element_type=jnp.float32
    )
    width = keys.shape[0]
    scores = (scores.reshape(heads, rows, width) + bias[None]).reshape(heads * rows, width)
    row_max = jnp.max(scores, axis=-1, keepdims=True)
    expo = jnp.exp(scores - row_max)
    denom = jnp.sum(expo, axis=-1, keepdims=True)
    summed = jnp.dot(expo.astype(jnp.bfloat16), values, preferred_element_type=jnp.float32)
    summed = summed / denom
    lse = row_max + jnp.log(denom)
    parts = [slice(head * rows, (head + 1) * rows) for head in range(heads)]
    out = sum(summed[part] * mask for part, mask in zip(parts, masks))
    return out, [lse[part] for part in parts]


def packed_lse(lses):
    heads = len(lses)
    lane = lax.broadcasted_iota(jnp.int32, (1, 128), 1)
    spread = sum(lse * (lane % heads == head).astype(jnp.float32) for head, lse in enumerate(lses))
    total = jnp.zeros_like(spread)
    for term in range(3):
        rounded = spread.astype(jnp.bfloat16).astype(jnp.float32)
        total = total + rounded * (lane // heads == term).astype(jnp.float32)
        spread = spread - rounded
    return total.astype(jnp.bfloat16)


def band_bias(rows, width, offset, low, high):
    query = lax.broadcasted_iota(jnp.int32, (rows, width), 0)
    key = lax.broadcasted_iota(jnp.int32, (rows, width), 1)
    step = key + offset - query
    keep = (step >= -SIDE_STEPS) & (step <= SIDE_STEPS) & (key >= low) & (key < high)
    return jnp.where(keep, 0.0, -1e30)


def permutation(length, dilation, inverse):
    row = lax.broadcasted_iota(jnp.int32, (length, length), 1 if inverse else 0)
    column = lax.broadcasted_iota(jnp.int32, (length, length), 0 if inverse else 1)
    steps = length // dilation
    source = (row % steps) * dilation + row // steps
    return (source == column).astype(jnp.float32).astype(jnp.bfloat16)


def fused_kernel(
    n, m, tokens_hbm, query_hbm, key_hbm, value_hbm, out_hbm, table_hbm, base_ref, result_ref,
    tokens, weights, out_weight, table, kv_first, kv_middle, far_send, far_recv,
    back_send, back_recv, merged_all, load_sem, weight_sem, local_sem,
    near_send_sem, near_recv_sem, far_send_sem, far_recv_sem, back_send_sem, back_recv_sem,
    tp_send_sem, tp_recv_sem,
):
    me = lax.axis_index("sp")
    mine = lax.axis_index("tp")
    length, columns = tokens.shape[0], weights.shape[-1]
    half = HEAD_DIM // 2
    classes = FAR_DILATION // n
    halo = SIDE_STEPS

    loads = [
        pltpu.make_async_copy(tokens_hbm, tokens, load_sem.at[0]),
        pltpu.make_async_copy(table_hbm, table, load_sem.at[1]),
        pltpu.make_async_copy(out_hbm, out_weight, load_sem.at[2]),
    ]
    weight_loads = {}
    for group in (2, 1, 0):
        for kind, source in ((1, key_hbm), (2, value_hbm), (0, query_hbm)):
            slot = group * 3 + kind
            weight_loads[group, kind] = pltpu.make_async_copy(
                source.at[group], weights.at[slot], weight_sem.at[slot]
            )
    loads[0].start()
    loads[1].start()
    for kind in (1, 2, 0):
        weight_loads[2, kind].start()
    later_loads = [weight_loads[group, kind] for group in (0, 1) for kind in (1, 2)]
    later_loads += [weight_loads[1, 0], weight_loads[0, 0], loads[2]]

    barrier = pltpu.get_barrier_semaphore()
    for distance in range(1, n):
        pl.semaphore_signal(
            barrier, inc=1, device_id={"sp": lax.rem(me + distance, n)}, device_id_type=MESH
        )
    for distance in range(1, m):
        pl.semaphore_signal(
            barrier, inc=1, device_id={"tp": lax.rem(mine + distance, m)}, device_id_type=MESH
        )

    @pl.when(me == 0)
    def _():
        kv_first[:, :halo] = jnp.zeros((2, halo, columns), jnp.bfloat16)
        kv_middle[:, :, 0] = jnp.zeros_like(kv_middle[:, :, 0])

    @pl.when(me == n - 1)
    def _():
        kv_first[:, halo + length :] = jnp.zeros((2, halo, columns), jnp.bfloat16)
        kv_middle[:, :, 2] = jnp.zeros_like(kv_middle[:, :, 2])

    loads[1].wait()
    base_cos = base_ref[0, pl.ds(me, 1), :]
    base_sin = base_ref[1, pl.ds(me, 1), :]
    cosine = base_cos * table[0] - base_sin * table[1]
    sine = base_sin * table[0] + base_cos * table[1]
    wide = columns // cosine.shape[1]
    lane = lax.broadcasted_iota(jnp.int32, (1, columns), 1)
    first_half = lane % HEAD_DIM < half
    cosine = jnp.concatenate([cosine] * wide, axis=1)
    sine = jnp.concatenate([sine] * wide, axis=1) * jnp.where(first_half, -1.0, 1.0)
    far_order = permutation(length, FAR_DILATION, False)
    middle_order = permutation(length, MIDDLE_DILATION, False)
    loads[0].wait()

    def project(group, kind):
        weight_loads[group, kind].wait()
        product = jnp.dot(
            tokens[...], weights[group * 3 + kind], preferred_element_type=jnp.float32
        )
        if kind < 2:
            later = pltpu.roll(product, columns - half, 1)
            earlier = pltpu.roll(product, half, 1)
            product = product * cosine + jnp.where(first_half, later, earlier) * sine
        if kind == 0:
            product = product * HEAD_DIM ** (-0.5)
        return product.astype(jnp.bfloat16)

    def ordered(order, block):
        return jnp.dot(order, block, preferred_element_type=jnp.float32).astype(jnp.bfloat16)

    far_copies = []
    for kind in (1, 2, 0):
        far_send[kind] = ordered(far_order, project(2, kind)).reshape(far_send.shape[1:])
        for load in later_loads[:3]:
            load.start()
        later_loads = later_loads[3:]
        if kind == 1:
            pl.semaphore_wait(barrier, n - 1 + m - 1)
        for distance in range(1, n):
            target = lax.rem(me + distance, n)
            copy = remote(
                far_send.at[kind, pl.ds(target * classes, classes)],
                far_recv.at[kind, :, me],
                far_send_sem.at[kind, distance],
                far_recv_sem.at[kind, distance],
                "sp",
                target,
            )
            copy.start()
            far_copies.append(copy)
    far_own = pltpu.make_async_copy(
        far_send.at[:, pl.ds(me * classes, classes)], far_recv.at[:, :, me], local_sem.at[0]
    )
    far_own.start()

    middle_up = remote(
        kv_middle.at[:, :, 1], kv_middle.at[:, :, 0],
        near_send_sem.at[0], near_recv_sem.at[0], "sp", lax.rem(me + 1, n),
    )
    middle_down = remote(
        kv_middle.at[:, :, 1], kv_middle.at[:, :, 2],
        near_send_sem.at[1], near_recv_sem.at[1], "sp", lax.rem(me + n - 1, n),
    )
    first_up = remote(
        kv_first.at[:, pl.ds(length, halo)], kv_first.at[:, pl.ds(0, halo)],
        near_send_sem.at[2], near_recv_sem.at[2], "sp", lax.rem(me + 1, n),
    )
    first_down = remote(
        kv_first.at[:, pl.ds(halo, halo)], kv_first.at[:, pl.ds(halo + length, halo)],
        near_send_sem.at[3], near_recv_sem.at[3], "sp", lax.rem(me + n - 1, n),
    )

    for kind in (1, 2):
        kv_first[kind - 1, halo : halo + length] = project(0, kind)

    @pl.when(me < n - 1)
    def _():
        first_up.start()

    @pl.when(me > 0)
    def _():
        first_down.start()

    for kind in (1, 2):
        kv_middle[kind - 1, :, 1] = ordered(middle_order, project(1, kind)).reshape(
            MIDDLE_DILATION, length // MIDDLE_DILATION, columns
        )
    @pl.when(me < n - 1)
    def _():
        middle_up.start()

    @pl.when(me > 0)
    def _():
        middle_down.start()

    middle_queries = ordered(middle_order, project(1, 0))
    first_queries = project(0, 0)

    far_own.wait()
    for copy in far_copies:
        copy.wait()
    class_len = n * (length // FAR_DILATION)
    far_bias = band_bias(class_len, class_len, 0, 0, class_len)
    for index in range(classes):
        queries, keys, values = (
            far_recv[kind, index].reshape(class_len, columns) for kind in range(3)
        )
        out, lses = attend(queries, keys, values, far_bias)
        back_send[index, :, :, :columns] = out.astype(jnp.bfloat16).reshape(n, -1, columns)
        back_send[index, :, :, columns:] = packed_lse(lses).reshape(n, -1, 128)
    back_copies = []
    for distance in range(1, n):
        target = lax.rem(me + distance, n)
        copy = remote(
            back_send.at[:, target],
            back_recv.at[pl.ds(me * classes, classes)],
            back_send_sem.at[distance],
            back_recv_sem.at[distance],
            "sp",
            target,
        )
        copy.start()
        back_copies.append(copy)
    back_own = pltpu.make_async_copy(
        back_send.at[:, me], back_recv.at[pl.ds(me * classes, classes)], local_sem.at[1]
    )
    back_own.start()

    @pl.when(me < n - 1)
    def _():
        first_up.wait_send()
        first_down.wait_recv()

    @pl.when(me > 0)
    def _():
        first_down.wait_send()
        first_up.wait_recv()

    tile = 2 * halo
    first_outs = []
    first_lses = []
    for start in range(0, length, tile):
        width = tile + 2 * halo
        low = halo - start - me * length
        high = halo - start + (n - me) * length
        out, lses = attend(
            first_queries[start : start + tile],
            kv_first[0, start : start + width],
            kv_first[1, start : start + width],
            band_bias(tile, width, -halo, low, high),
        )
        first_outs.append(out)
        first_lses.append(
            sum(lse * head_mask(columns, head) for head, lse in enumerate(lses))
        )
    first_out = jnp.concatenate(first_outs, axis=0)
    first_lse = jnp.concatenate(first_lses, axis=0)

    @pl.when(me < n - 1)
    def _():
        middle_up.wait_send()
        middle_down.wait_recv()

    @pl.when(me > 0)
    def _():
        middle_down.wait_send()
        middle_up.wait_recv()

    steps = length // MIDDLE_DILATION
    low = jnp.where(me == 0, steps, 0)
    high = jnp.where(me == n - 1, 2 * steps, 3 * steps)
    middle_bias = band_bias(steps, 3 * steps, -steps, low, high)
    middle_parts = []
    for index in range(MIDDLE_DILATION):
        out, lses = attend(
            middle_queries[index * steps : (index + 1) * steps],
            kv_middle[0, index].reshape(3 * steps, columns),
            kv_middle[1, index].reshape(3 * steps, columns),
            middle_bias,
        )
        middle_parts.append(
            jnp.concatenate([out.astype(jnp.bfloat16), packed_lse(lses)], axis=1)
        )

    heads = columns // HEAD_DIM
    term = lax.broadcasted_iota(jnp.int32, (128, columns), 0)
    column = lax.broadcasted_iota(jnp.int32, (128, columns), 1)
    spread = (term % heads == column // HEAD_DIM) & (term < 3 * heads)
    spread = spread.astype(jnp.float32).astype(jnp.bfloat16)

    def natural(dilation, block):
        block = jnp.dot(
            permutation(length, dilation, True), block, preferred_element_type=jnp.float32
        )
        lse = jnp.dot(
            block[:, columns:].astype(jnp.bfloat16), spread, preferred_element_type=jnp.float32
        )
        return block[:, :columns], lse

    middle_out, middle_lse = natural(MIDDLE_DILATION, jnp.concatenate(middle_parts, axis=0))

    back_own.wait()
    for copy in back_copies:
        copy.wait()
    far_out, far_lse = natural(
        FAR_DILATION, back_recv[...].reshape(length, back_recv.shape[2])
    )

    top = jnp.maximum(jnp.maximum(first_lse, middle_lse), far_lse)
    first_w = jnp.exp(first_lse - top)
    middle_w = jnp.exp(middle_lse - top)
    far_w = jnp.exp(far_lse - top)
    merged = (first_w * first_out + middle_w * middle_out + far_w * far_out) / (
        first_w + middle_w + far_w
    )
    merged_all[0] = merged.astype(jnp.bfloat16)

    chips = m // 2
    sibling = mine + 1 - 2 * lax.rem(mine, 2)
    piece = length // 2

    def hand(part, source, slot, target):
        rows = pl.ds(part * piece, piece)
        copy = remote(
            merged_all.at[source, rows],
            merged_all.at[slot, rows],
            tp_send_sem.at[part, slot],
            tp_recv_sem.at[part, slot],
            "tp",
            target,
        )
        copy.start()
        return copy

    copies = {}
    for part in range(2):
        for chip in range(1, chips):
            copies[part, chip] = hand(part, 0, chip, lax.rem(mine + 2 * chip, m))
    for part in range(2):
        copies[part, chips] = hand(part, 0, chips, sibling)
    loads[2].wait()

    def term(part, slot):
        chip = slot % chips
        owner = lax.rem((mine if slot < chips else sibling) - 2 * chip + m, m)
        rows = pl.ds(pl.multiple_of(owner * columns, columns), columns)
        return jnp.dot(
            merged_all[slot, part * piece : (part + 1) * piece],
            out_weight[rows, :],
            preferred_element_type=jnp.float32,
        )

    totals = [term(part, 0) for part in range(2)]
    for part in range(2):
        for chip in range(1, chips):
            copies[part, chip].wait()
            copies[part, chips + chip] = hand(part, chip, chips + chip, sibling)
        copies[part, chips].wait()
        totals[part] = totals[part] + term(part, chips)
        for chip in range(1, chips):
            totals[part] = totals[part] + term(part, chip)
    for part in range(2):
        for chip in range(1, chips):
            copies[part, chips + chip].wait()
            totals[part] = totals[part] + term(part, chips + chip)
        result_ref[part * piece : (part + 1) * piece] = totals[part].astype(result_ref.dtype)


def turn_tables(n, length):
    half = HEAD_DIM // 2
    inverse = 1.0 / 10000.0 ** (np.arange(half, dtype=np.float32) * np.float32(2.0) / HEAD_DIM)
    inverse = np.tile(inverse.astype(np.float64), 128 // half)[None]
    inner = np.arange(length)[:, None] * inverse
    outer = (np.arange(n) * length)[:, None] * inverse
    table = np.stack([np.cos(inner), np.sin(inner)]).astype(np.float32)
    base = np.stack([np.cos(outer), np.sin(outer)]).astype(np.float32)
    return table, base


def fused(n, m, tokens, query_weight, key_weight, value_weight, out_weight):
    length, width = tokens.shape
    columns = query_weight.shape[2]
    table, base = turn_tables(n, length)
    steps = length // FAR_DILATION
    classes = FAR_DILATION // n
    kept = columns + 128
    bf16 = jnp.bfloat16
    hbm = pl.BlockSpec(memory_space=pl.ANY)
    vmem = pl.BlockSpec(memory_space=pltpu.VMEM)
    dma = pltpu.SemaphoreType.DMA
    return pl.pallas_call(
        functools.partial(fused_kernel, n, m),
        out_shape=jax.ShapeDtypeStruct((length, out_weight.shape[1]), jnp.float32),
        in_specs=[hbm] * 6 + [vmem],
        out_specs=vmem,
        scratch_shapes=[
            pltpu.VMEM((length, width), bf16),
            pltpu.VMEM((9, width, columns), bf16),
            pltpu.VMEM(out_weight.shape, bf16),
            pltpu.VMEM(table.shape, jnp.float32),
            pltpu.VMEM((2, length + 2 * SIDE_STEPS, columns), bf16),
            pltpu.VMEM((2, MIDDLE_DILATION, 3, length // MIDDLE_DILATION, columns), bf16),
            pltpu.VMEM((3, FAR_DILATION, steps, columns), bf16),
            pltpu.VMEM((3, classes, n, steps, columns), bf16),
            pltpu.VMEM((classes, n, steps, kept), bf16),
            pltpu.VMEM((FAR_DILATION, steps, kept), bf16),
            pltpu.VMEM((m, length, columns), bf16),
            dma((3,)),
            dma((9,)),
            dma((2,)),
            dma((4,)),
            dma((4,)),
            dma((3, n)),
            dma((3, n)),
            dma((n,)),
            dma((n,)),
            dma((2, m)),
            dma((2, m)),
        ],
        compiler_params=pltpu.CompilerParams(
            collective_id=0, has_side_effects=True, vmem_limit_bytes=60 * 1024 * 1024
        ),
    )(tokens, query_weight, key_weight, value_weight, out_weight, jnp.asarray(table), jnp.asarray(base)).astype(bf16)


def planned(n, m, *arrays):
    length, columns = arrays[0].shape[0], arrays[1].shape[2]
    fits = (
        n > 1
        and m % 2 == 0
        and FAR_DILATION % n == 0
        and length == SIDE_STEPS * MIDDLE_DILATION
        and length % (FAR_DILATION * 16) == 0
        and columns % 128 == 0
        and 3 * (columns // HEAD_DIM) <= 128
    )
    if fits:
        return fused(n, m, *arrays)
    return per_device(*arrays)


def solution(mesh):
    placed = (
        P("sp", None),
        P(None, None, "tp"),
        P(None, None, "tp"),
        P(None, None, "tp"),
        P(None, "tp"),
    )
    return jax.shard_map(
        functools.partial(planned, mesh.shape["sp"], mesh.shape["tp"]),
        mesh=mesh,
        in_specs=placed,
        out_specs=P("sp", "tp"),
        check_vma=False,
    )
```

profile of v0, /device:TPU:1, one launch (start us, length us, event | category | flops | bytes accessed | tf_op | source)
XLA Modules:
  0.0 38.4 jit_solution(5307375031878666694)
XLA Ops:
  0.0 36.6 %shard_map.73 = f32[256,512]{1,0:T(8,128)} custom-call(bf16[256,2048]{1,0:T(8,128)(2,1)} %tokens_hbm.1, bf16[3,2048,256]{2,1,0:T(8,128)(2,1)} %query_hbm.1, bf16[3,2048,256]{2,1,0:T(8,128)(2,1)} %key_hbm.1, bf16[3,2048,256]{2,1,0:T(8,128)(2,1)} %value_hbm.1, bf16[1024,512]{1,0:T(8,128)(2,1)} %out_hbm.1, f32[2,256,128]{2,1,0:T(8,128)} %constant.4.clone.table_hbm, ...), custom_call_target="tpu_custom_call" | custom-call | tf_op jit(solution)/shard_map/pallas_call | solution.py:573
  36.6 1.8 %convert_element_type.3 = bf16[256,512]{1,0:T(8,128)(2,1)} convert(f32[256,512]{1,0:T(8,128)} %shard_map.73) | non-fusion elementwise | flops 131072 | bytes 786432 | tf_op jit(solution)/shard_map/convert_element_type | solution.py:605
where the time goes:
time: 39 us; the launch traced here: 38.4 us
  Pallas kernels  36.6 us (94%)
  other arithmetic  1.78 us (5%)
    pallas_call x1, Pallas kernels, fused(): pl.pallas_call(functools.partial(fused_kernel, n, m), out_shape=jax.Shape...  36.6 us
    convert_element_type x1, other arithmetic, fused(): return pl.pallas_call(functools.partial(fused_kernel, n, m), out_shape=ja...  1.78 us

commit v1 on v0

--- a/solution.py
+++ b/solution.py
@@ -572,7 +572,7 @@
     dma = pltpu.SemaphoreType.DMA
     return pl.pallas_call(
         functools.partial(fused_kernel, n, m),
-        out_shape=jax.ShapeDtypeStruct((length, out_weight.shape[1]), jnp.float32),
+        out_shape=pltpu.VMEM((length, out_weight.shape[1]), bf16),
         in_specs=[hbm] * 6 + [vmem],
         out_specs=vmem,
         scratch_shapes=[
@@ -602,7 +602,7 @@
         compiler_params=pltpu.CompilerParams(
             collective_id=0, has_side_effects=True, vmem_limit_bytes=60 * 1024 * 1024
         ),
-    )(tokens, query_weight, key_weight, value_weight, out_weight, jnp.asarray(table), jnp.asarray(base)).astype(bf16)
+    )(tokens, query_weight, key_weight, value_weight, out_weight, jnp.asarray(table), jnp.asarray(base))
 
 
 def planned(n, m, *arrays):

time: 39 us -> 37.2 us (0.954)
  other arithmetic: 1.78 us -> 0 us
  Pallas kernels: 36.6 us -> 35.8 us
  local copies, waits for them, and re-layouts: 0 us -> 0.71 us
    convert_element_type x1 -> x0, other arithmetic: 1.78 us -> none  [fused(): return pl.pallas_call(functools.partial(fused_kernel, n, m), out_shape=ja...]
    pallas_call x1, Pallas kernels: 36.6 us -> 35.8 us  [fused(): pl.pallas_call(functools.partial(fused_kernel, n, m), out_shape=pltpu.VME...]
    unnamed x0 -> x1, local copies, waits for them, and re-layouts: none -> 0.71 us
where the time goes in v1:
time: 37.2 us; the launch traced here: 36.5 us
  Pallas kernels  35.8 us (96%)
  local copies, waits for them, and re-layouts  0.71 us (2%)
    pallas_call x1, Pallas kernels, fused(): pl.pallas_call(functools.partial(fused_kernel, n, m), out_shape=pltpu.VME...  35.8 us

profile of v1, /device:TPU:1, one launch (start us, length us, event | category | flops | bytes accessed | tf_op | source)
XLA Modules:
  0.0 36.5 jit_solution(17408069860308738717)
XLA Ops:
  0.0 35.8 %shard_map.73 = bf16[256,512]{1,0:T(8,128)(2,1)S(1)} custom-call(bf16[256,2048]{1,0:T(8,128)(2,1)} %tokens_hbm.1, bf16[3,2048,256]{2,1,0:T(8,128)(2,1)} %query_hbm.1, bf16[3,2048,256]{2,1,0:T(8,128)(2,1)} %key_hbm.1, bf16[3,2048,256]{2,1,0:T(8,128)(2,1)} %value_hbm.1, bf16[1024,512]{1,0:T(8,128)(2,1)} %out_hbm.1, f32[2,256,128]{2,1,0:T(8,128)} %constant.4.clone.table_hbm, ...), custom_call_target="tpu_custom_call" | custom-call | tf_op jit(solution)/shard_map/pallas_call | solution.py:573
  35.8 0.7 %copy.9 = bf16[256,512]{1,0:T(8,128)(2,1)} copy(bf16[256,512]{1,0:T(8,128)(2,1)S(1)} %shard_map.73) | data formatting | bytes 524288

commit v2 on v1

--- a/solution.py
+++ b/solution.py
@@ -211,54 +211,92 @@
     return total.astype(jnp.bfloat16)
 
 
-def band_bias(rows, width, offset, low, high):
+def in_terms(block):
+    terms = []
+    for _ in range(3):
+        rounded = block.astype(jnp.bfloat16)
+        terms.append(rounded)
+        block = block - rounded.astype(jnp.float32)
+    return jnp.concatenate(terms, axis=1)
+
+
+def band_bias(rows, width, offset, low, high, stride=1):
     query = lax.broadcasted_iota(jnp.int32, (rows, width), 0)
     key = lax.broadcasted_iota(jnp.int32, (rows, width), 1)
+    query = (query % (rows // stride)) * stride + query // (rows // stride)
     step = key + offset - query
     keep = (step >= -SIDE_STEPS) & (step <= SIDE_STEPS) & (key >= low) & (key < high)
     return jnp.where(keep, 0.0, -1e30)
 
 
-def permutation(length, dilation, inverse):
-    row = lax.broadcasted_iota(jnp.int32, (length, length), 1 if inverse else 0)
-    column = lax.broadcasted_iota(jnp.int32, (length, length), 0 if inverse else 1)
-    steps = length // dilation
-    source = (row % steps) * dilation + row // steps
-    return (source == column).astype(jnp.float32).astype(jnp.bfloat16)
+def one_hot(size, source_of_row):
+    row = lax.broadcasted_iota(jnp.int32, (size, size), 0)
+    column = lax.broadcasted_iota(jnp.int32, (size, size), 1)
+    return (source_of_row(row) == column).astype(jnp.float32).astype(jnp.bfloat16)
+
+
+def scope(name):
+    return jax.named_scope(name)
 
 
 def fused_kernel(
-    n, m, tokens_hbm, query_hbm, key_hbm, value_hbm, out_hbm, table_hbm, base_ref, result_ref,
-    tokens, weights, out_weight, table, kv_first, kv_middle, far_send, far_recv,
-    back_send, back_recv, merged_all, load_sem, weight_sem, local_sem,
-    near_send_sem, near_recv_sem, far_send_sem, far_recv_sem, back_send_sem, back_recv_sem,
+    n, m, tokens_hbm, query_hbm, key_hbm, value_hbm, out_hbm, table_hbm, base_hbm, result_ref,
+    tokens, weights, out_weight, table, base, kv_first, mid_kv, mid_q, mid_send, mid_ret,
+    mid_back, far_send, far_recv, back_send, back_recv, lse_send, lse_recv, merged_all,
+    result_wide, load_sem, weight_sem, local_sem, first_send_sem, first_recv_sem,
+    pair_send_sem, pair_recv_sem, hop_send_sem, hop_recv_sem, ret_send_sem, ret_recv_sem,
+    far_send_sem, far_recv_sem, back_send_sem, back_recv_sem, lse_send_sem, lse_recv_sem,
     tp_send_sem, tp_recv_sem,
 ):
     me = lax.axis_index("sp")
     mine = lax.axis_index("tp")
+    side = lax.rem(me, 2)
+    partner = me + 1 - 2 * side
     length, columns = tokens.shape[0], weights.shape[-1]
+    depth = tokens.shape[1]
+    heads = columns // HEAD_DIM
     half = HEAD_DIM // 2
     classes = FAR_DILATION // n
+    far_steps = length // FAR_DILATION
     halo = SIDE_STEPS
-
-    loads = [
-        pltpu.make_async_copy(tokens_hbm, tokens, load_sem.at[0]),
-        pltpu.make_async_copy(table_hbm, table, load_sem.at[1]),
-        pltpu.make_async_copy(out_hbm, out_weight, load_sem.at[2]),
-    ]
+    steps = length // MIDDLE_DILATION
+    piece = length // 2
+
+    chunk = depth // 2
+    token_loads = []
+    first_loads = []
+    for index in range(2):
+        part = pl.ds(index * chunk, chunk)
+        token_loads.append(
+            pltpu.make_async_copy(tokens_hbm.at[:, part], tokens.at[:, part], load_sem.at[index])
+        )
+        first_loads.append(
+            pltpu.make_async_copy(
+                key_hbm.at[2, part], weights.at[2 * 3 + 1, part], load_sem.at[2 + index]
+            )
+        )
+    table_load = pltpu.make_async_copy(table_hbm, table, load_sem.at[4])
+    base_load = pltpu.make_async_copy(base_hbm, base, load_sem.at[5])
+    out_load = pltpu.make_async_copy(out_hbm, out_weight, load_sem.at[6])
     weight_loads = {}
     for group in (2, 1, 0):
         for kind, source in ((1, key_hbm), (2, value_hbm), (0, query_hbm)):
             slot = group * 3 + kind
+            if (group, kind) == (2, 1):
+                continue
             weight_loads[group, kind] = pltpu.make_async_copy(
                 source.at[group], weights.at[slot], weight_sem.at[slot]
             )
-    loads[0].start()
-    loads[1].start()
-    for kind in (1, 2, 0):
-        weight_loads[2, kind].start()
-    later_loads = [weight_loads[group, kind] for group in (0, 1) for kind in (1, 2)]
-    later_loads += [weight_loads[1, 0], weight_loads[0, 0], loads[2]]
+    token_loads[0].start()
+    first_loads[0].start()
+    base_load.start()
+    table_load.start()
+    token_loads[1].start()
+    first_loads[1].start()
+    weight_loads[2, 2].start()
+    weight_loads[2, 0].start()
+    later_loads = [weight_loads[group, kind] for group in (1, 0) for kind in (1, 2, 0)]
+    later_loads.append(out_load)
 
     barrier = pltpu.get_barrier_semaphore()
     for distance in range(1, n):
@@ -270,54 +308,78 @@
             barrier, inc=1, device_id={"tp": lax.rem(mine + distance, m)}, device_id_type=MESH
         )
 
-    @pl.when(me == 0)
-    def _():
-        kv_first[:, :halo] = jnp.zeros((2, halo, columns), jnp.bfloat16)
-        kv_middle[:, :, 0] = jnp.zeros_like(kv_middle[:, :, 0])
-
-    @pl.when(me == n - 1)
-    def _():
-        kv_first[:, halo + length :] = jnp.zeros((2, halo, columns), jnp.bfloat16)
-        kv_middle[:, :, 2] = jnp.zeros_like(kv_middle[:, :, 2])
-
-    loads[1].wait()
-    base_cos = base_ref[0, pl.ds(me, 1), :]
-    base_sin = base_ref[1, pl.ds(me, 1), :]
-    cosine = base_cos * table[0] - base_sin * table[1]
-    sine = base_sin * table[0] + base_cos * table[1]
-    wide = columns // cosine.shape[1]
+    far_order = one_hot(
+        length, lambda row: (row % far_steps) * FAR_DILATION + row // far_steps
+    )
+    middle_order = one_hot(
+        length,
+        lambda row: (row % steps) * MIDDLE_DILATION + (row // steps + 2 * side) % MIDDLE_DILATION,
+    )
+    tile = 2 * halo
+    first_order = one_hot(
+        length, lambda row: row // tile * tile + (row % halo) * 2 + row % tile // halo
+    )
     lane = lax.broadcasted_iota(jnp.int32, (1, columns), 1)
     first_half = lane % HEAD_DIM < half
-    cosine = jnp.concatenate([cosine] * wide, axis=1)
-    sine = jnp.concatenate([sine] * wide, axis=1) * jnp.where(first_half, -1.0, 1.0)
-    far_order = permutation(length, FAR_DILATION, False)
-    middle_order = permutation(length, MIDDLE_DILATION, False)
-    loads[0].wait()
-
-    def project(group, kind):
-        weight_loads[group, kind].wait()
-        product = jnp.dot(
-            tokens[...], weights[group * 3 + kind], preferred_element_type=jnp.float32
-        )
+
+    def product_of(slot, low, size):
+        return jnp.dot(
+            tokens[:, low : low + size],
+            weights[slot, low : low + size],
+            preferred_element_type=jnp.float32,
+        )
+
+    def rolled(block, shift):
+        return jnp.concatenate(
+            [pltpu.roll(block[:, at : at + 128], shift, 1) for at in range(0, columns, 128)], axis=1
+        )
+
+    def turned(product, kind):
         if kind < 2:
-            later = pltpu.roll(product, columns - half, 1)
-            earlier = pltpu.roll(product, half, 1)
+            later = rolled(product, 128 - half)
+            earlier = rolled(product, half)
             product = product * cosine + jnp.where(first_half, later, earlier) * sine
         if kind == 0:
             product = product * HEAD_DIM ** (-0.5)
         return product.astype(jnp.bfloat16)
 
+    def project(group, kind):
+        slot = group * 3 + kind
+        weight_loads[group, kind].wait()
+        return turned(product_of(slot, 0, depth), kind)
+
     def ordered(order, block):
         return jnp.dot(order, block, preferred_element_type=jnp.float32).astype(jnp.bfloat16)
 
+    with scope("w_load0"):
+        token_loads[0].wait()
+        first_loads[0].wait()
+    first_product = product_of(7, 0, chunk)
+    with scope("w_load1"):
+        base_load.wait()
+        table_load.wait()
+        token_loads[1].wait()
+        first_loads[1].wait()
+    first_product = first_product + product_of(7, chunk, chunk)
+    base_cos = base[0, pl.ds(me, 1), :]
+    base_sin = base[1, pl.ds(me, 1), :]
+    cosine = base_cos * table[0] - base_sin * table[1]
+    sine = base_sin * table[0] + base_cos * table[1]
+    wide = columns // cosine.shape[1]
+    cosine = jnp.concatenate([cosine] * wide, axis=1)
+    sine = jnp.concatenate([sine] * wide, axis=1) * jnp.where(first_half, -1.0, 1.0)
+
     far_copies = []
     for kind in (1, 2, 0):
-        far_send[kind] = ordered(far_order, project(2, kind)).reshape(far_send.shape[1:])
+        with scope(f"p_far{kind}"):
+            block = turned(first_product, 1) if kind == 1 else project(2, kind)
+            far_send[kind] = ordered(far_order, block).reshape(far_send.shape[1:])
         for load in later_loads[:3]:
             load.start()
         later_loads = later_loads[3:]
         if kind == 1:
-            pl.semaphore_wait(barrier, n - 1 + m - 1)
+            with scope("w_barrier"):
+                pl.semaphore_wait(barrier, n - 1 + m - 1)
         for distance in range(1, n):
             target = lax.rem(me + distance, n)
             copy = remote(
@@ -335,25 +397,52 @@
     )
     far_own.start()
 
-    middle_up = remote(
-        kv_middle.at[:, :, 1], kv_middle.at[:, :, 0],
-        near_send_sem.at[0], near_recv_sem.at[0], "sp", lax.rem(me + 1, n),
-    )
-    middle_down = remote(
-        kv_middle.at[:, :, 1], kv_middle.at[:, :, 2],
-        near_send_sem.at[1], near_recv_sem.at[1], "sp", lax.rem(me + n - 1, n),
-    )
+    pair_copies = []
+    for kind in (1, 2, 0):
+        with scope(f"p_mid{kind}"):
+            block = ordered(middle_order, project(1, kind)).reshape(2, 2, steps, columns)
+            if kind == 0:
+                mid_q[:, pl.ds(side, 1)] = block[0][:, None]
+                landing = mid_q.at[:, side]
+            else:
+                mid_kv[kind - 1, :, pl.ds(1 + side, 1)] = block[0][:, None]
+                landing = mid_kv.at[kind - 1, :, 1 + side]
+            mid_send[kind] = block[1]
+        copy = remote(
+            mid_send.at[kind], landing, pair_send_sem.at[kind], pair_recv_sem.at[kind],
+            "sp", partner,
+        )
+        copy.start()
+        pair_copies.append(copy)
+
+    for kind in (1, 2):
+        with scope(f"p_first{kind}"):
+            kv_first[kind - 1, halo : halo + length] = project(0, kind)
+
+    @pl.when(me == 0)
+    def _():
+        kv_first[:, :halo] = jnp.zeros((2, halo, columns), jnp.bfloat16)
+
+    @pl.when(me == n - 1)
+    def _():
+        kv_first[:, halo + length :] = jnp.zeros((2, halo, columns), jnp.bfloat16)
+
+    @pl.when(me < 2)
+    def _():
+        mid_kv[:, :, 0] = jnp.zeros_like(mid_kv[:, :, 0])
+
+    @pl.when(me >= n - 2)
+    def _():
+        mid_kv[:, :, 3] = jnp.zeros_like(mid_kv[:, :, 3])
+
     first_up = remote(
         kv_first.at[:, pl.ds(length, halo)], kv_first.at[:, pl.ds(0, halo)],
-        near_send_sem.at[2], near_recv_sem.at[2], "sp", lax.rem(me + 1, n),
+        first_send_sem.at[0], first_recv_sem.at[0], "sp", lax.rem(me + 1, n),
     )
     first_down = remote(
         kv_first.at[:, pl.ds(halo, halo)], kv_first.at[:, pl.ds(halo + length, halo)],
-        near_send_sem.at[3], near_recv_sem.at[3], "sp", lax.rem(me + n - 1, n),
-    )
-
-    for kind in (1, 2):
-        kv_first[kind - 1, halo : halo + length] = project(0, kind)
+        first_send_sem.at[1], first_recv_sem.at[1], "sp", lax.rem(me + n - 1, n),
+    )
 
     @pl.when(me < n - 1)
     def _():
@@ -363,143 +452,177 @@
     def _():
         first_down.start()
 
-    for kind in (1, 2):
-        kv_middle[kind - 1, :, 1] = ordered(middle_order, project(1, kind)).reshape(
-            MIDDLE_DILATION, length // MIDDLE_DILATION, columns
-        )
-    @pl.when(me < n - 1)
+    with scope("p_first0"):
+        first_queries = ordered(first_order, project(0, 0))
+
+    hop_up = remote(
+        mid_kv.at[:, :, 2], mid_kv.at[:, :, 0],
+        hop_send_sem.at[0], hop_recv_sem.at[0], "sp", lax.rem(me + 2, n),
+    )
+    hop_down = remote(
+        mid_kv.at[:, :, 1], mid_kv.at[:, :, 3],
+        hop_send_sem.at[1], hop_recv_sem.at[1], "sp", lax.rem(me + n - 2, n),
+    )
+    with scope("w_pair"):
+        pair_copies[0].wait_recv()
+        pair_copies[1].wait_recv()
+
+    @pl.when(me < n - 2)
     def _():
-        middle_up.start()
-
-    @pl.when(me > 0)
+        hop_up.start()
+
+    @pl.when(me >= 2)
     def _():
-        middle_down.start()
-
-    middle_queries = ordered(middle_order, project(1, 0))
-    first_queries = project(0, 0)
-
-    far_own.wait()
-    for copy in far_copies:
-        copy.wait()
-    class_len = n * (length // FAR_DILATION)
+        hop_down.start()
+
+    with scope("w_far"):
+        far_own.wait()
+        for copy in far_copies:
+            copy.wait()
+    class_len = n * far_steps
     far_bias = band_bias(class_len, class_len, 0, 0, class_len)
+    row16 = lax.broadcasted_iota(jnp.int32, (class_len, 128), 0) % far_steps
+    lane16 = lax.broadcasted_iota(jnp.int32, (class_len, 128), 1)
+    diagonal = lane16 % far_steps == row16
+    back_copies = []
     for index in range(classes):
-        queries, keys, values = (
-            far_recv[kind, index].reshape(class_len, columns) for kind in range(3)
-        )
-        out, lses = attend(queries, keys, values, far_bias)
-        back_send[index, :, :, :columns] = out.astype(jnp.bfloat16).reshape(n, -1, columns)
-        back_send[index, :, :, columns:] = packed_lse(lses).reshape(n, -1, 128)
-    back_copies = []
-    for distance in range(1, n):
-        target = lax.rem(me + distance, n)
-        copy = remote(
-            back_send.at[:, target],
-            back_recv.at[pl.ds(me * classes, classes)],
-            back_send_sem.at[distance],
-            back_recv_sem.at[distance],
-            "sp",
-            target,
-        )
-        copy.start()
-        back_copies.append(copy)
-    back_own = pltpu.make_async_copy(
-        back_send.at[:, me], back_recv.at[pl.ds(me * classes, classes)], local_sem.at[1]
-    )
-    back_own.start()
-
-    @pl.when(me < n - 1)
-    def _():
-        first_up.wait_send()
-        first_down.wait_recv()
-
-    @pl.when(me > 0)
-    def _():
-        first_down.wait_send()
-        first_up.wait_recv()
-
-    tile = 2 * halo
+        with scope(f"c_far{index}"):
+            queries, keys, values = (
+                far_recv[kind, index].reshape(class_len, columns) for kind in range(3)
+            )
+            out, lses = attend(queries, keys, values, far_bias)
+            back_send[index] = out.astype(jnp.bfloat16).reshape(n, far_steps, columns)
+            spread = sum(
+                jnp.where(diagonal & (lane16 // far_steps == head), lse, 0.0)
+                for head, lse in enumerate(lses)
+            )
+            lse_send[index] = jnp.sum(spread.reshape(n, far_steps, 128), axis=1, keepdims=True)
+        sent = []
+        for distance in range(1, n):
+            target = lax.rem(me + distance, n)
+            for source, landing, send_sem, recv_sem in (
+                (back_send, back_recv, back_send_sem, back_recv_sem),
+                (lse_send, lse_recv, lse_send_sem, lse_recv_sem),
+            ):
+                copy = remote(
+                    source.at[index, target], landing.at[index, me],
+                    send_sem.at[index, distance], recv_sem.at[index, distance], "sp", target,
+                )
+                copy.start()
+                sent.append(copy)
+        for which, (source, landing) in enumerate(((back_send, back_recv), (lse_send, lse_recv))):
+            copy = pltpu.make_async_copy(
+                source.at[index, me], landing.at[index, me], local_sem.at[1 + 2 * index + which]
+            )
+            copy.start()
+            sent.append(copy)
+        back_copies.append(sent)
+
+    with scope("w_first"):
+        @pl.when(me < n - 1)
+        def _():
+            first_up.wait_send()
+            first_down.wait_recv()
+
+        @pl.when(me > 0)
+        def _():
+            first_down.wait_send()
+            first_up.wait_recv()
+
     first_outs = []
     first_lses = []
-    for start in range(0, length, tile):
-        width = tile + 2 * halo
-        low = halo - start - me * length
-        high = halo - start + (n - me) * length
-        out, lses = attend(
-            first_queries[start : start + tile],
-            kv_first[0, start : start + width],
-            kv_first[1, start : start + width],
-            band_bias(tile, width, -halo, low, high),
-        )
-        first_outs.append(out)
-        first_lses.append(
-            sum(lse * head_mask(columns, head) for head, lse in enumerate(lses))
-        )
-    first_out = jnp.concatenate(first_outs, axis=0)
-    first_lse = jnp.concatenate(first_lses, axis=0)
-
-    @pl.when(me < n - 1)
-    def _():
-        middle_up.wait_send()
-        middle_down.wait_recv()
-
-    @pl.when(me > 0)
-    def _():
-        middle_down.wait_send()
-        middle_up.wait_recv()
-
-    steps = length // MIDDLE_DILATION
-    low = jnp.where(me == 0, steps, 0)
-    high = jnp.where(me == n - 1, 2 * steps, 3 * steps)
-    middle_bias = band_bias(steps, 3 * steps, -steps, low, high)
-    middle_parts = []
-    for index in range(MIDDLE_DILATION):
-        out, lses = attend(
-            middle_queries[index * steps : (index + 1) * steps],
-            kv_middle[0, index].reshape(3 * steps, columns),
-            kv_middle[1, index].reshape(3 * steps, columns),
-            middle_bias,
-        )
-        middle_parts.append(
-            jnp.concatenate([out.astype(jnp.bfloat16), packed_lse(lses)], axis=1)
-        )
-
-    heads = columns // HEAD_DIM
-    term = lax.broadcasted_iota(jnp.int32, (128, columns), 0)
+    with scope("c_first"):
+        for start in range(0, length, tile):
+            width = tile + 2 * halo
+            low = halo - start - me * length
+            high = halo - start + (n - me) * length
+            out, lses = attend(
+                first_queries[start : start + tile],
+                kv_first[0, start : start + width],
+                kv_first[1, start : start + width],
+                band_bias(tile, width, -halo, low, high, 2),
+            )
+            first_outs.append(out)
+            first_lses.append(
+                sum(lse * head_mask(columns, head) for head, lse in enumerate(lses))
+            )
+
+    with scope("w_hop"):
+        pair_copies[2].wait_recv()
+        for copy in pair_copies:
+            copy.wait_send()
+
+        @pl.when(me < n - 2)
+        def _():
+            hop_up.wait_send()
+            hop_down.wait_recv()
+
+        @pl.when(me >= 2)
+        def _():
+            hop_down.wait_send()
+            hop_up.wait_recv()
+
+    low = jnp.where(me < 2, steps, 0)
+    high = jnp.where(me >= n - 2, 3 * steps, 4 * steps)
+    middle_bias = band_bias(2 * steps, 4 * steps, -steps, low, high)
+    ret_copies = []
+    for index in range(2):
+        with scope(f"c_mid{index}"):
+            out, lses = attend(
+                mid_q[index].reshape(2 * steps, columns),
+                mid_kv[0, index].reshape(4 * steps, columns),
+                mid_kv[1, index].reshape(4 * steps, columns),
+                middle_bias,
+            )
+            mid_ret[index] = jnp.concatenate(
+                [out.astype(jnp.bfloat16), packed_lse(lses)], axis=1
+            ).reshape(2, steps, columns + 128)
+        copy = remote(
+            mid_ret.at[index, 1 - side], mid_back.at[index],
+            ret_send_sem.at[index], ret_recv_sem.at[index], "sp", partner,
+        )
+        copy.start()
+        ret_copies.append(copy)
+
+    term_row = lax.broadcasted_iota(jnp.int32, (128, columns), 0)
     column = lax.broadcasted_iota(jnp.int32, (128, columns), 1)
-    spread = (term % heads == column // HEAD_DIM) & (term < 3 * heads)
-    spread = spread.astype(jnp.float32).astype(jnp.bfloat16)
-
-    def natural(dilation, block):
-        block = jnp.dot(
-            permutation(length, dilation, True), block, preferred_element_type=jnp.float32
-        )
-        lse = jnp.dot(
-            block[:, columns:].astype(jnp.bfloat16), spread, preferred_element_type=jnp.float32
-        )
-        return block[:, :columns], lse
-
-    middle_out, middle_lse = natural(MIDDLE_DILATION, jnp.concatenate(middle_parts, axis=0))
-
-    back_own.wait()
-    for copy in back_copies:
-        copy.wait()
-    far_out, far_lse = natural(
-        FAR_DILATION, back_recv[...].reshape(length, back_recv.shape[2])
-    )
-
-    top = jnp.maximum(jnp.maximum(first_lse, middle_lse), far_lse)
-    first_w = jnp.exp(first_lse - top)
-    middle_w = jnp.exp(middle_lse - top)
-    far_w = jnp.exp(far_lse - top)
-    merged = (first_w * first_out + middle_w * middle_out + far_w * far_out) / (
-        first_w + middle_w + far_w
-    )
-    merged_all[0] = merged.astype(jnp.bfloat16)
+    middle_spread = (term_row % heads == column // HEAD_DIM) & (term_row < 3 * heads)
+    middle_spread = middle_spread.astype(jnp.float32).astype(jnp.bfloat16)
+    far_spread = term_row // far_steps == column // HEAD_DIM
+    far_spread = far_spread.astype(jnp.float32).astype(jnp.bfloat16)
+    far_spread = jnp.concatenate([far_spread] * 3, axis=0)
+    middle_natural = one_hot(
+        piece, lambda row: row // 2 + steps * ((row % 2 + side) % 2)
+    )
+    far_natural = one_hot(piece, lambda row: (row % n) * far_steps + row // n)
+    position = lax.broadcasted_iota(jnp.int32, (piece, 128), 0) // n
+    lane_part = lax.broadcasted_iota(jnp.int32, (piece, 128), 1)
+    far_keep = (lane_part % far_steps == position) & (lane_part < heads * far_steps)
+
+    near = []
+    for part in range(2):
+        with scope(f"w_ret{part}"):
+            ret_copies[part].wait()
+        with scope(f"c_near{part}"):
+            block = jnp.concatenate([mid_ret[part, side], mid_back[part]], axis=0)
+            block = jnp.dot(middle_natural, block, preferred_element_type=jnp.float32)
+            middle_lse = jnp.dot(
+                block[:, columns:].astype(jnp.bfloat16),
+                middle_spread,
+                preferred_element_type=jnp.float32,
+            )
+            rows = slice(part * halo, (part + 1) * halo)
+            first_out = jnp.concatenate([out[rows] for out in first_outs], axis=0)
+            first_lse = jnp.concatenate([lse[rows] for lse in first_lses], axis=0)
+            top = jnp.maximum(first_lse, middle_lse)
+            first_w = jnp.exp(first_lse - top)
+            middle_w = jnp.exp(middle_lse - top)
+            near.append(
+                (first_w * first_out + middle_w * block[:, :columns], first_w + middle_w, top)
+            )
 
     chips = m // 2
     sibling = mine + 1 - 2 * lax.rem(mine, 2)
-    piece = length // 2
 
     def hand(part, source, slot, target):
         rows = pl.ds(part * piece, piece)
@@ -514,14 +637,6 @@
         copy.start()
         return copy
 
-    copies = {}
-    for part in range(2):
-        for chip in range(1, chips):
-            copies[part, chip] = hand(part, 0, chip, lax.rem(mine + 2 * chip, m))
-    for part in range(2):
-        copies[part, chips] = hand(part, 0, chips, sibling)
-    loads[2].wait()
-
     def term(part, slot):
         chip = slot % chips
         owner = lax.rem((mine if slot < chips else sibling) - 2 * chip + m, m)
@@ -532,20 +647,57 @@
             preferred_element_type=jnp.float32,
         )
 
-    totals = [term(part, 0) for part in range(2)]
+    copies = {}
+    totals = []
+    with scope("w_outw"):
+        out_load.wait()
+    for part in range(2):
+        with scope(f"w_back{part}"):
+            for copy in back_copies[part]:
+                copy.wait()
+        with scope(f"c_merge{part}"):
+            far_out = jnp.dot(
+                far_natural,
+                back_recv[part].reshape(piece, columns),
+                preferred_element_type=jnp.float32,
+            )
+            lse = jnp.concatenate([lse_recv[part].reshape(n, 128)] * (piece // n), axis=0)
+            lse = jnp.where(far_keep, lse, 0.0)
+            far_lse = jnp.dot(in_terms(lse), far_spread, preferred_element_type=jnp.float32)
+            total, weight, near_top = near[part]
+            top = jnp.maximum(near_top, far_lse)
+            near_w = jnp.exp(near_top - top)
+            far_w = jnp.exp(far_lse - top)
+            merged = (near_w * total + far_w * far_out) / (near_w * weight + far_w)
+            merged_all[0, part * piece : (part + 1) * piece] = merged.astype(jnp.bfloat16)
+        for chip in range(1, chips):
+            copies[part, chip] = hand(part, 0, chip, lax.rem(mine + 2 * chip, m))
+        copies[part, chips] = hand(part, 0, chips, sibling)
+        totals.append(term(part, 0))
+
     for part in range(2):
         for chip in range(1, chips):
-            copies[part, chip].wait()
+            with scope(f"w_chip{part}"):
+                copies[part, chip].wait()
             copies[part, chips + chip] = hand(part, chip, chips + chip, sibling)
-        copies[part, chips].wait()
+        with scope(f"w_sib{part}"):
+            copies[part, chips].wait()
         totals[part] = totals[part] + term(part, chips)
         for chip in range(1, chips):
             totals[part] = totals[part] + term(part, chip)
     for part in range(2):
         for chip in range(1, chips):
-            copies[part, chips + chip].wait()
+            with scope(f"w_fwd{part}"):
+                copies[part, chips + chip].wait()
             totals[part] = totals[part] + term(part, chips + chip)
-        result_ref[part * piece : (part + 1) * piece] = totals[part].astype(result_ref.dtype)
+        for index in range(result_wide.shape[0]):
+            result_wide[index, pl.ds(part, piece, stride=2), :] = totals[part][
+                :, index * 128 : (index + 1) * 128
+            ]
+    for index in range(result_wide.shape[0]):
+        result_ref[:, index * 128 : (index + 1) * 128] = result_wide[index].astype(
+            result_ref.dtype
+        )
 
 
 def turn_tables(n, length):
@@ -564,6 +716,7 @@
     columns = query_weight.shape[2]
     table, base = turn_tables(n, length)
     steps = length // FAR_DILATION
+    span = length // MIDDLE_DILATION
     classes = FAR_DILATION // n
     kept = columns + 128
     bf16 = jnp.bfloat16
@@ -573,29 +726,45 @@
     return pl.pallas_call(
         functools.partial(fused_kernel, n, m),
         out_shape=pltpu.VMEM((length, out_weight.shape[1]), bf16),
-        in_specs=[hbm] * 6 + [vmem],
+        in_specs=[hbm] * 7,
         out_specs=vmem,
         scratch_shapes=[
             pltpu.VMEM((length, width), bf16),
             pltpu.VMEM((9, width, columns), bf16),
             pltpu.VMEM(out_weight.shape, bf16),
             pltpu.VMEM(table.shape, jnp.float32),
+            pltpu.VMEM(base.shape, jnp.float32),
             pltpu.VMEM((2, length + 2 * SIDE_STEPS, columns), bf16),
-            pltpu.VMEM((2, MIDDLE_DILATION, 3, length // MIDDLE_DILATION, columns), bf16),
+            pltpu.VMEM((2, 2, 4, span, columns), bf16),
+            pltpu.VMEM((2, 2, span, columns), bf16),
+            pltpu.VMEM((3, 2, span, columns), bf16),
+            pltpu.VMEM((2, 2, span, kept), bf16),
+            pltpu.VMEM((2, span, kept), bf16),
             pltpu.VMEM((3, FAR_DILATION, steps, columns), bf16),
             pltpu.VMEM((3, classes, n, steps, columns), bf16),
-            pltpu.VMEM((classes, n, steps, kept), bf16),
-            pltpu.VMEM((FAR_DILATION, steps, kept), bf16),
+            pltpu.VMEM((classes, n, steps, columns), bf16),
+            pltpu.VMEM((classes, n, steps, columns), bf16),
+            pltpu.VMEM((classes, n, 1, 128), jnp.float32),
+            pltpu.VMEM((classes, n, 1, 128), jnp.float32),
             pltpu.VMEM((m, length, columns), bf16),
+            pltpu.VMEM((out_weight.shape[1] // 128, length, 128), jnp.float32),
+            dma((7,)),
+            dma((9,)),
+            dma((1 + 2 * classes,)),
+            dma((2,)),
+            dma((2,)),
             dma((3,)),
-            dma((9,)),
+            dma((3,)),
             dma((2,)),
-            dma((4,)),
-            dma((4,)),
+            dma((2,)),
+            dma((2,)),
+            dma((2,)),
             dma((3, n)),
             dma((3, n)),
-            dma((n,)),
-            dma((n,)),
+            dma((classes, n)),
+            dma((classes, n)),
+            dma((classes, n)),
+            dma((classes, n)),
             dma((2, m)),
             dma((2, m)),
         ],
@@ -608,13 +777,16 @@
 def planned(n, m, *arrays):
     length, columns = arrays[0].shape[0], arrays[1].shape[2]
     fits = (
-        n > 1
+        n == 8
         and m % 2 == 0
-        and FAR_DILATION % n == 0
+        and FAR_DILATION == 2 * n
+        and MIDDLE_DILATION == 4
         and length == SIDE_STEPS * MIDDLE_DILATION
         and length % (FAR_DILATION * 16) == 0
         and columns % 128 == 0
+        and arrays[4].shape[1] % 128 == 0
         and 3 * (columns // HEAD_DIM) <= 128
+        and columns // HEAD_DIM * (length // FAR_DILATION) <= 128
     )
     if fits:
         return fused(n, m, *arrays)

time: 37.2 us -> 33.9 us (0.911); the launches traced: 36.5 us -> 33.6 us
  Pallas kernels: 35.8 us -> 32.9 us
    pallas_call x1, Pallas kernels: 35.8 us -> 32.9 us  [fused(): pl.pallas_call(functools.partial(fused_kernel, n, m), out_shape=pltpu.VME...]
where the time goes in v2:
time: 33.9 us; the launch traced here: 33.6 us
  Pallas kernels  32.9 us (97%)
  local copies, waits for them, and re-layouts  0.71 us (2%)
    pallas_call x1, Pallas kernels, fused(): pl.pallas_call(functools.partial(fused_kernel, n, m), out_shape=pltpu.VME...  32.9 us
    unnamed x1, local copies, waits for them, and re-layouts  0.71 us

profile of v2, /device:TPU:1, one launch (start us, length us, event | category | flops | bytes accessed | tf_op | source)
XLA Modules:
  0.0 33.6 jit_solution(11463715249972930260)
XLA Ops:
  0.0 32.9 %shard_map.73 = bf16[256,512]{1,0:T(8,128)(2,1)S(1)} custom-call(bf16[256,2048]{1,0:T(8,128)(2,1)} %tokens_hbm.1, bf16[3,2048,256]{2,1,0:T(8,128)(2,1)} %query_hbm.1, bf16[3,2048,256]{2,1,0:T(8,128)(2,1)} %key_hbm.1, bf16[3,2048,256]{2,1,0:T(8,128)(2,1)} %value_hbm.1, bf16[1024,512]{1,0:T(8,128)(2,1)} %out_hbm.1, f32[2,256,128]{2,1,0:T(8,128)} %constant.4.clone.table_hbm, ...), custom_call_target="tpu_custom_call" | custom-call | tf_op jit(solution)/shard_map/pallas_call | solution.py:726
  32.9 0.7 %copy.9 = bf16[256,512]{1,0:T(8,128)(2,1)} copy(bf16[256,512]{1,0:T(8,128)(2,1)S(1)} %shard_map.73) | data formatting | bytes 524288

commit v3 on v2

--- a/solution.py
+++ b/solution.py
@@ -199,18 +199,6 @@
     return out, [lse[part] for part in parts]
 
 
-def packed_lse(lses):
-    heads = len(lses)
-    lane = lax.broadcasted_iota(jnp.int32, (1, 128), 1)
-    spread = sum(lse * (lane % heads == head).astype(jnp.float32) for head, lse in enumerate(lses))
-    total = jnp.zeros_like(spread)
-    for term in range(3):
-        rounded = spread.astype(jnp.bfloat16).astype(jnp.float32)
-        total = total + rounded * (lane // heads == term).astype(jnp.float32)
-        spread = spread - rounded
-    return total.astype(jnp.bfloat16)
-
-
 def in_terms(block):
     terms = []
     for _ in range(3):
@@ -239,14 +227,16 @@
     return jax.named_scope(name)
 
 
+def take(ref, sem):
+    pltpu.make_async_copy(ref, ref, sem).wait()
+
+
 def fused_kernel(
-    n, m, tokens_hbm, query_hbm, key_hbm, value_hbm, out_hbm, table_hbm, base_hbm, result_ref,
-    tokens, weights, out_weight, table, base, kv_first, mid_kv, mid_q, mid_send, mid_ret,
-    mid_back, far_send, far_recv, back_send, back_recv, lse_send, lse_recv, merged_all,
-    result_wide, load_sem, weight_sem, local_sem, first_send_sem, first_recv_sem,
-    pair_send_sem, pair_recv_sem, hop_send_sem, hop_recv_sem, ret_send_sem, ret_recv_sem,
-    far_send_sem, far_recv_sem, back_send_sem, back_recv_sem, lse_send_sem, lse_recv_sem,
-    tp_send_sem, tp_recv_sem,
+    n, m, tokens_hbm, query_hbm, key_hbm, value_hbm, out_hbm, table_hbm, result_ref,
+    tokens, weights, out_weight, table, kv_first, mid_kv, mid_q, mid_send, mid_ret, mid_back,
+    mid_lse, mid_lse_back, far_send, far_recv, back_send, back_recv, lse_send, lse_recv,
+    merged_all, result_wide, load_sem, weight_sem, first_sem, pair_sem, hop_sem, ret_sem,
+    far_sem, back_sem, tp_send_sem, tp_recv_sem,
 ):
     me = lax.axis_index("sp")
     mine = lax.axis_index("tp")
@@ -261,42 +251,31 @@
     halo = SIDE_STEPS
     steps = length // MIDDLE_DILATION
     piece = length // 2
-
-    chunk = depth // 2
-    token_loads = []
-    first_loads = []
-    for index in range(2):
+    sub = steps // 8
+
+    table_load = pltpu.make_async_copy(table_hbm, table, load_sem.at[0])
+    table_load.start()
+    chunks = 4
+    chunk = depth // chunks
+    for index in range(chunks):
         part = pl.ds(index * chunk, chunk)
-        token_loads.append(
-            pltpu.make_async_copy(tokens_hbm.at[:, part], tokens.at[:, part], load_sem.at[index])
-        )
-        first_loads.append(
-            pltpu.make_async_copy(
-                key_hbm.at[2, part], weights.at[2 * 3 + 1, part], load_sem.at[2 + index]
-            )
-        )
-    table_load = pltpu.make_async_copy(table_hbm, table, load_sem.at[4])
-    base_load = pltpu.make_async_copy(base_hbm, base, load_sem.at[5])
-    out_load = pltpu.make_async_copy(out_hbm, out_weight, load_sem.at[6])
+        sem = load_sem.at[1 + index]
+        pltpu.make_async_copy(tokens_hbm.at[:, part], tokens.at[:, part], sem).start()
+        pltpu.make_async_copy(key_hbm.at[2, part], weights.at[7, part], sem).start()
+    out_load = pltpu.make_async_copy(out_hbm, out_weight, load_sem.at[1 + chunks])
+    sources = (query_hbm, key_hbm, value_hbm)
+    order = ((2, 2), (2, 0), (1, 1), (1, 2), (1, 0), (0, 1), (0, 2), (0, 0))
+    waiting = []
     weight_loads = {}
-    for group in (2, 1, 0):
-        for kind, source in ((1, key_hbm), (2, value_hbm), (0, query_hbm)):
-            slot = group * 3 + kind
-            if (group, kind) == (2, 1):
-                continue
-            weight_loads[group, kind] = pltpu.make_async_copy(
-                source.at[group], weights.at[slot], weight_sem.at[slot]
-            )
-    token_loads[0].start()
-    first_loads[0].start()
-    base_load.start()
-    table_load.start()
-    token_loads[1].start()
-    first_loads[1].start()
-    weight_loads[2, 2].start()
-    weight_loads[2, 0].start()
-    later_loads = [weight_loads[group, kind] for group in (1, 0) for kind in (1, 2, 0)]
-    later_loads.append(out_load)
+    for index, (group, kind) in enumerate(order):
+        slot = group * 3 + kind
+        load = pltpu.make_async_copy(
+            sources[kind].at[group], weights.at[slot], weight_sem.at[index % 4]
+        )
+        weight_loads[group, kind] = load
+        waiting.append(load)
+    waiting.append(out_load)
+    waiting.pop(0).start()
 
     barrier = pltpu.get_barrier_semaphore()
     for distance in range(1, n):
@@ -346,59 +325,52 @@
     def project(group, kind):
         slot = group * 3 + kind
         weight_loads[group, kind].wait()
+        if waiting:
+            waiting.pop(0).start()
         return turned(product_of(slot, 0, depth), kind)
 
     def ordered(order, block):
         return jnp.dot(order, block, preferred_element_type=jnp.float32).astype(jnp.bfloat16)
 
-    with scope("w_load0"):
-        token_loads[0].wait()
-        first_loads[0].wait()
-    first_product = product_of(7, 0, chunk)
-    with scope("w_load1"):
-        base_load.wait()
+    with scope("w_table"):
         table_load.wait()
-        token_loads[1].wait()
-        first_loads[1].wait()
-    first_product = first_product + product_of(7, chunk, chunk)
-    base_cos = base[0, pl.ds(me, 1), :]
-    base_sin = base[1, pl.ds(me, 1), :]
-    cosine = base_cos * table[0] - base_sin * table[1]
-    sine = base_sin * table[0] + base_cos * table[1]
+    base_cos = table[0, pl.ds(length + me, 1), :]
+    base_sin = table[1, pl.ds(length + me, 1), :]
+    inner_cos = table[0, 0:length]
+    inner_sin = table[1, 0:length]
+    cosine = base_cos * inner_cos - base_sin * inner_sin
+    sine = base_sin * inner_cos + base_cos * inner_sin
     wide = columns // cosine.shape[1]
     cosine = jnp.concatenate([cosine] * wide, axis=1)
     sine = jnp.concatenate([sine] * wide, axis=1) * jnp.where(first_half, -1.0, 1.0)
-
-    far_copies = []
-    for kind in (1, 2, 0):
+    first_product = None
+    for index in range(chunks):
+        with scope(f"w_load{index}"):
+            take(weights.at[7, pl.ds(0, 2 * chunk)], load_sem.at[1 + index])
+        term = product_of(7, index * chunk, chunk)
+        first_product = term if first_product is None else first_product + term
+    for _ in range(3):
+        waiting.pop(0).start()
+
+    def far(kind):
         with scope(f"p_far{kind}"):
             block = turned(first_product, 1) if kind == 1 else project(2, kind)
             far_send[kind] = ordered(far_order, block).reshape(far_send.shape[1:])
-        for load in later_loads[:3]:
-            load.start()
-        later_loads = later_loads[3:]
         if kind == 1:
             with scope("w_barrier"):
                 pl.semaphore_wait(barrier, n - 1 + m - 1)
         for distance in range(1, n):
             target = lax.rem(me + distance, n)
-            copy = remote(
+            remote(
                 far_send.at[kind, pl.ds(target * classes, classes)],
-                far_recv.at[kind, :, me],
-                far_send_sem.at[kind, distance],
-                far_recv_sem.at[kind, distance],
-                "sp",
-                target,
-            )
-            copy.start()
-            far_copies.append(copy)
-    far_own = pltpu.make_async_copy(
-        far_send.at[:, pl.ds(me * classes, classes)], far_recv.at[:, :, me], local_sem.at[0]
-    )
-    far_own.start()
-
-    pair_copies = []
-    for kind in (1, 2, 0):
+                far_recv.at[kind, :, me], far_sem.at[0], far_sem.at[1], "sp", target,
+            ).start()
+        pltpu.make_async_copy(
+            far_send.at[kind, pl.ds(me * classes, classes)], far_recv.at[kind, :, me],
+            far_sem.at[1],
+        ).start()
+
+    def middle(kind):
         with scope(f"p_mid{kind}"):
             block = ordered(middle_order, project(1, kind)).reshape(2, 2, steps, columns)
             if kind == 0:
@@ -408,17 +380,56 @@
                 mid_kv[kind - 1, :, pl.ds(1 + side, 1)] = block[0][:, None]
                 landing = mid_kv.at[kind - 1, :, 1 + side]
             mid_send[kind] = block[1]
-        copy = remote(
-            mid_send.at[kind], landing, pair_send_sem.at[kind], pair_recv_sem.at[kind],
+        remote(
+            mid_send.at[kind], landing, pair_sem.at[0], pair_sem.at[1 if kind else 2],
             "sp", partner,
-        )
-        copy.start()
-        pair_copies.append(copy)
+        ).start()
+
+    lean = 2 * side - 1
+    has_ahead = (me + 2 * lean >= 0) & (me + 2 * lean < n)
+    has_behind = (me - 2 * lean >= 0) & (me - 2 * lean < n)
+    direct = remote(
+        mid_kv.at[:, :, 1 + side], mid_kv.at[:, :, 3 * (1 - side)],
+        hop_sem.at[0], hop_sem.at[1], "sp", lax.rem(me + 2 * lean + n, n),
+    )
+    relay = remote(
+        mid_kv.at[:, :, 2 - side], mid_kv.at[:, :, 3 * side],
+        hop_sem.at[2], hop_sem.at[3], "sp", lax.rem(me - 2 * lean + n, n),
+    )
+
+    far(1)
+    far(2)
+    far(0)
+    middle(1)
+    middle(2)
+
+    @pl.when(has_ahead)
+    def _():
+        direct.start()
+
+    middle(0)
 
     for kind in (1, 2):
         with scope(f"p_first{kind}"):
             kv_first[kind - 1, halo : halo + length] = project(0, kind)
 
+    first_up = remote(
+        kv_first.at[:, pl.ds(length, halo)], kv_first.at[:, pl.ds(0, halo)],
+        first_sem.at[0], first_sem.at[1], "sp", lax.rem(me + 1, n),
+    )
+    first_down = remote(
+        kv_first.at[:, pl.ds(halo, halo)], kv_first.at[:, pl.ds(halo + length, halo)],
+        first_sem.at[2], first_sem.at[3], "sp", lax.rem(me + n - 1, n),
+    )
+
+    @pl.when(me < n - 1)
+    def _():
+        first_up.start()
+
+    @pl.when(me > 0)
+    def _():
+        first_down.start()
+
     @pl.when(me == 0)
     def _():
         kv_first[:, :halo] = jnp.zeros((2, halo, columns), jnp.bfloat16)
@@ -435,56 +446,23 @@
     def _():
         mid_kv[:, :, 3] = jnp.zeros_like(mid_kv[:, :, 3])
 
-    first_up = remote(
-        kv_first.at[:, pl.ds(length, halo)], kv_first.at[:, pl.ds(0, halo)],
-        first_send_sem.at[0], first_recv_sem.at[0], "sp", lax.rem(me + 1, n),
-    )
-    first_down = remote(
-        kv_first.at[:, pl.ds(halo, halo)], kv_first.at[:, pl.ds(halo + length, halo)],
-        first_send_sem.at[1], first_recv_sem.at[1], "sp", lax.rem(me + n - 1, n),
-    )
-
-    @pl.when(me < n - 1)
-    def _():
-        first_up.start()
-
-    @pl.when(me > 0)
-    def _():
-        first_down.start()
-
     with scope("p_first0"):
         first_queries = ordered(first_order, project(0, 0))
 
-    hop_up = remote(
-        mid_kv.at[:, :, 2], mid_kv.at[:, :, 0],
-        hop_send_sem.at[0], hop_recv_sem.at[0], "sp", lax.rem(me + 2, n),
-    )
-    hop_down = remote(
-        mid_kv.at[:, :, 1], mid_kv.at[:, :, 3],
-        hop_send_sem.at[1], hop_recv_sem.at[1], "sp", lax.rem(me + n - 2, n),
-    )
     with scope("w_pair"):
-        pair_copies[0].wait_recv()
-        pair_copies[1].wait_recv()
-
-    @pl.when(me < n - 2)
+        take(mid_kv.at[:, :, 2 - side], pair_sem.at[1])
+
+    @pl.when(has_behind)
     def _():
-        hop_up.start()
-
-    @pl.when(me >= 2)
-    def _():
-        hop_down.start()
+        relay.start()
 
     with scope("w_far"):
-        far_own.wait()
-        for copy in far_copies:
-            copy.wait()
+        take(far_recv, far_sem.at[1])
     class_len = n * far_steps
     far_bias = band_bias(class_len, class_len, 0, 0, class_len)
     row16 = lax.broadcasted_iota(jnp.int32, (class_len, 128), 0) % far_steps
     lane16 = lax.broadcasted_iota(jnp.int32, (class_len, 128), 1)
     diagonal = lane16 % far_steps == row16
-    back_copies = []
     for index in range(classes):
         with scope(f"c_far{index}"):
             queries, keys, values = (
@@ -497,26 +475,54 @@
                 for head, lse in enumerate(lses)
             )
             lse_send[index] = jnp.sum(spread.reshape(n, far_steps, 128), axis=1, keepdims=True)
-        sent = []
-        for distance in range(1, n):
-            target = lax.rem(me + distance, n)
-            for source, landing, send_sem, recv_sem in (
-                (back_send, back_recv, back_send_sem, back_recv_sem),
-                (lse_send, lse_recv, lse_send_sem, lse_recv_sem),
-            ):
-                copy = remote(
+        for which, (source, landing) in enumerate(((back_send, back_recv), (lse_send, lse_recv))):
+            for distance in range(1, n):
+                target = lax.rem(me + distance, n)
+                remote(
                     source.at[index, target], landing.at[index, me],
-                    send_sem.at[index, distance], recv_sem.at[index, distance], "sp", target,
-                )
-                copy.start()
-                sent.append(copy)
-        for which, (source, landing) in enumerate(((back_send, back_recv), (lse_send, lse_recv))):
-            copy = pltpu.make_async_copy(
-                source.at[index, me], landing.at[index, me], local_sem.at[1 + 2 * index + which]
-            )
-            copy.start()
-            sent.append(copy)
-        back_copies.append(sent)
+                    back_sem.at[which], back_sem.at[2 + 2 * index + which], "sp", target,
+                ).start()
+            pltpu.make_async_copy(
+                source.at[index, me], landing.at[index, me], back_sem.at[2 + 2 * index + which]
+            ).start()
+
+    with scope("w_hop"):
+        take(mid_q.at[:, 1 - side], pair_sem.at[2])
+
+        @pl.when(has_ahead)
+        def _():
+            direct.wait_send()
+            relay.wait_recv()
+
+        @pl.when(has_behind)
+        def _():
+            relay.wait_send()
+            direct.wait_recv()
+
+    low = jnp.where(me < 2, steps, 0)
+    high = jnp.where(me >= n - 2, 3 * steps, 4 * steps)
+    middle_bias = band_bias(2 * steps, 4 * steps, -steps, low, high)
+    sub_row = lax.broadcasted_iota(jnp.int32, (2 * steps, 128), 0) % steps // 8
+    sub_lane = lax.broadcasted_iota(jnp.int32, (2 * steps, 128), 1)
+    for index in range(2):
+        with scope(f"c_mid{index}"):
+            out, lses = attend(
+                mid_q[index].reshape(2 * steps, columns),
+                mid_kv[0, index].reshape(4 * steps, columns),
+                mid_kv[1, index].reshape(4 * steps, columns),
+                middle_bias,
+            )
+            mid_ret[index] = out.astype(jnp.bfloat16).reshape(2, steps, columns)
+            spread = sum(
+                jnp.where((sub_lane % sub == sub_row) & (sub_lane // sub == head), lse, 0.0)
+                for head, lse in enumerate(lses)
+            )
+            mid_lse[index] = jnp.sum(spread.reshape(2, sub, 8, 128), axis=1)
+        for which, (source, landing) in enumerate(((mid_ret, mid_back), (mid_lse, mid_lse_back))):
+            remote(
+                source.at[index, 1 - side], landing.at[index],
+                ret_sem.at[which], ret_sem.at[2 + 2 * index + which], "sp", partner,
+            ).start()
 
     with scope("w_first"):
         @pl.when(me < n - 1)
@@ -547,50 +553,14 @@
                 sum(lse * head_mask(columns, head) for head, lse in enumerate(lses))
             )
 
-    with scope("w_hop"):
-        pair_copies[2].wait_recv()
-        for copy in pair_copies:
-            copy.wait_send()
-
-        @pl.when(me < n - 2)
-        def _():
-            hop_up.wait_send()
-            hop_down.wait_recv()
-
-        @pl.when(me >= 2)
-        def _():
-            hop_down.wait_send()
-            hop_up.wait_recv()
-
-    low = jnp.where(me < 2, steps, 0)
-    high = jnp.where(me >= n - 2, 3 * steps, 4 * steps)
-    middle_bias = band_bias(2 * steps, 4 * steps, -steps, low, high)
-    ret_copies = []
-    for index in range(2):
-        with scope(f"c_mid{index}"):
-            out, lses = attend(
-                mid_q[index].reshape(2 * steps, columns),
-                mid_kv[0, index].reshape(4 * steps, columns),
-                mid_kv[1, index].reshape(4 * steps, columns),
-                middle_bias,
-            )
-            mid_ret[index] = jnp.concatenate(
-                [out.astype(jnp.bfloat16), packed_lse(lses)], axis=1
-            ).reshape(2, steps, columns + 128)
-        copy = remote(
-            mid_ret.at[index, 1 - side], mid_back.at[index],
-            ret_send_sem.at[index], ret_recv_sem.at[index], "sp", partner,
-        )
-        copy.start()
-        ret_copies.append(copy)
-
-    term_row = lax.broadcasted_iota(jnp.int32, (128, columns), 0)
-    column = lax.broadcasted_iota(jnp.int32, (128, columns), 1)
-    middle_spread = (term_row % heads == column // HEAD_DIM) & (term_row < 3 * heads)
-    middle_spread = middle_spread.astype(jnp.float32).astype(jnp.bfloat16)
-    far_spread = term_row // far_steps == column // HEAD_DIM
-    far_spread = far_spread.astype(jnp.float32).astype(jnp.bfloat16)
-    far_spread = jnp.concatenate([far_spread] * 3, axis=0)
+    def lane_spread(group):
+        term = lax.broadcasted_iota(jnp.int32, (128, columns), 0)
+        column = lax.broadcasted_iota(jnp.int32, (128, columns), 1)
+        keep = (term // group == column // HEAD_DIM).astype(jnp.float32).astype(jnp.bfloat16)
+        return jnp.concatenate([keep] * 3, axis=0)
+
+    middle_spread = lane_spread(sub)
+    far_spread = lane_spread(far_steps)
     middle_natural = one_hot(
         piece, lambda row: row // 2 + steps * ((row % 2 + side) % 2)
     )
@@ -598,18 +568,23 @@
     position = lax.broadcasted_iota(jnp.int32, (piece, 128), 0) // n
     lane_part = lax.broadcasted_iota(jnp.int32, (piece, 128), 1)
     far_keep = (lane_part % far_steps == position) & (lane_part < heads * far_steps)
+    middle_keep = (sub_lane % sub == sub_row) & (sub_lane < heads * sub)
 
     near = []
     for part in range(2):
         with scope(f"w_ret{part}"):
-            ret_copies[part].wait()
+            take(mid_back.at[part], ret_sem.at[2 + 2 * part])
+            take(mid_lse_back.at[part], ret_sem.at[3 + 2 * part])
         with scope(f"c_near{part}"):
             block = jnp.concatenate([mid_ret[part, side], mid_back[part]], axis=0)
             block = jnp.dot(middle_natural, block, preferred_element_type=jnp.float32)
+            lse = jnp.concatenate(
+                [mid_lse[part, side]] * sub + [mid_lse_back[part]] * sub, axis=0
+            )
+            lse = in_terms(jnp.where(middle_keep, lse, 0.0))
+            lse = jnp.dot(middle_natural, lse, preferred_element_type=jnp.float32)
             middle_lse = jnp.dot(
-                block[:, columns:].astype(jnp.bfloat16),
-                middle_spread,
-                preferred_element_type=jnp.float32,
+                lse.astype(jnp.bfloat16), middle_spread, preferred_element_type=jnp.float32
             )
             rows = slice(part * halo, (part + 1) * halo)
             first_out = jnp.concatenate([out[rows] for out in first_outs], axis=0)
@@ -617,9 +592,7 @@
             top = jnp.maximum(first_lse, middle_lse)
             first_w = jnp.exp(first_lse - top)
             middle_w = jnp.exp(middle_lse - top)
-            near.append(
-                (first_w * first_out + middle_w * block[:, :columns], first_w + middle_w, top)
-            )
+            near.append((first_w * first_out + middle_w * block, first_w + middle_w, top))
 
     chips = m // 2
     sibling = mine + 1 - 2 * lax.rem(mine, 2)
@@ -627,12 +600,8 @@
     def hand(part, source, slot, target):
         rows = pl.ds(part * piece, piece)
         copy = remote(
-            merged_all.at[source, rows],
-            merged_all.at[slot, rows],
-            tp_send_sem.at[part, slot],
-            tp_recv_sem.at[part, slot],
-            "tp",
-            target,
+            merged_all.at[source, rows], merged_all.at[slot, rows],
+            tp_send_sem.at[0], tp_recv_sem.at[part, slot - 1], "tp", target,
         )
         copy.start()
         return copy
@@ -653,8 +622,8 @@
         out_load.wait()
     for part in range(2):
         with scope(f"w_back{part}"):
-            for copy in back_copies[part]:
-                copy.wait()
+            take(back_recv.at[part], back_sem.at[2 + 2 * part])
+            take(lse_recv.at[part], back_sem.at[3 + 2 * part])
         with scope(f"c_merge{part}"):
             far_out = jnp.dot(
                 far_natural,
@@ -675,20 +644,27 @@
         copies[part, chips] = hand(part, 0, chips, sibling)
         totals.append(term(part, 0))
 
+    take(mid_send, pair_sem.at[0])
+    take(far_send.at[:, pl.ds(0, FAR_DILATION - classes)], far_sem.at[0])
+    take(back_send.at[:, pl.ds(0, n - 1)], back_sem.at[0])
+    take(lse_send.at[:, pl.ds(0, n - 1)], back_sem.at[1])
+    take(mid_back, ret_sem.at[0])
+    take(mid_lse_back, ret_sem.at[1])
+
     for part in range(2):
         for chip in range(1, chips):
             with scope(f"w_chip{part}"):
-                copies[part, chip].wait()
+                copies[part, chip].wait_recv()
             copies[part, chips + chip] = hand(part, chip, chips + chip, sibling)
         with scope(f"w_sib{part}"):
-            copies[part, chips].wait()
+            copies[part, chips].wait_recv()
         totals[part] = totals[part] + term(part, chips)
         for chip in range(1, chips):
             totals[part] = totals[part] + term(part, chip)
     for part in range(2):
         for chip in range(1, chips):
             with scope(f"w_fwd{part}"):
-                copies[part, chips + chip].wait()
+                copies[part, chips + chip].wait_recv()
             totals[part] = totals[part] + term(part, chips + chip)
         for index in range(result_wide.shape[0]):
             result_wide[index, pl.ds(part, piece, stride=2), :] = totals[part][
@@ -698,27 +674,25 @@
         result_ref[:, index * 128 : (index + 1) * 128] = result_wide[index].astype(
             result_ref.dtype
         )
+    take(merged_all.at[pl.ds(1, m - 1)], tp_send_sem.at[0])
 
 
 def turn_tables(n, length):
     half = HEAD_DIM // 2
     inverse = 1.0 / 10000.0 ** (np.arange(half, dtype=np.float32) * np.float32(2.0) / HEAD_DIM)
     inverse = np.tile(inverse.astype(np.float64), 128 // half)[None]
-    inner = np.arange(length)[:, None] * inverse
-    outer = (np.arange(n) * length)[:, None] * inverse
-    table = np.stack([np.cos(inner), np.sin(inner)]).astype(np.float32)
-    base = np.stack([np.cos(outer), np.sin(outer)]).astype(np.float32)
-    return table, base
+    positions = np.concatenate([np.arange(length), np.arange(n) * length])
+    angles = positions[:, None] * inverse
+    return np.stack([np.cos(angles), np.sin(angles)]).astype(np.float32)
 
 
 def fused(n, m, tokens, query_weight, key_weight, value_weight, out_weight):
     length, width = tokens.shape
     columns = query_weight.shape[2]
-    table, base = turn_tables(n, length)
+    table = turn_tables(n, length)
     steps = length // FAR_DILATION
     span = length // MIDDLE_DILATION
     classes = FAR_DILATION // n
-    kept = columns + 128
     bf16 = jnp.bfloat16
     hbm = pl.BlockSpec(memory_space=pl.ANY)
     vmem = pl.BlockSpec(memory_space=pltpu.VMEM)
@@ -726,20 +700,21 @@
     return pl.pallas_call(
         functools.partial(fused_kernel, n, m),
         out_shape=pltpu.VMEM((length, out_weight.shape[1]), bf16),
-        in_specs=[hbm] * 7,
+        in_specs=[hbm] * 6,
         out_specs=vmem,
         scratch_shapes=[
             pltpu.VMEM((length, width), bf16),
             pltpu.VMEM((9, width, columns), bf16),
             pltpu.VMEM(out_weight.shape, bf16),
             pltpu.VMEM(table.shape, jnp.float32),
-            pltpu.VMEM(base.shape, jnp.float32),
             pltpu.VMEM((2, length + 2 * SIDE_STEPS, columns), bf16),
             pltpu.VMEM((2, 2, 4, span, columns), bf16),
             pltpu.VMEM((2, 2, span, columns), bf16),
             pltpu.VMEM((3, 2, span, columns), bf16),
-            pltpu.VMEM((2, 2, span, kept), bf16),
-            pltpu.VMEM((2, span, kept), bf16),
+            pltpu.VMEM((2, 2, span, columns), bf16),
+            pltpu.VMEM((2, span, columns), bf16),
+            pltpu.VMEM((2, 2, 8, 128), jnp.float32),
+            pltpu.VMEM((2, 8, 128), jnp.float32),
             pltpu.VMEM((3, FAR_DILATION, steps, columns), bf16),
             pltpu.VMEM((3, classes, n, steps, columns), bf16),
             pltpu.VMEM((classes, n, steps, columns), bf16),
@@ -748,30 +723,21 @@
             pltpu.VMEM((classes, n, 1, 128), jnp.float32),
             pltpu.VMEM((m, length, columns), bf16),
             pltpu.VMEM((out_weight.shape[1] // 128, length, 128), jnp.float32),
-            dma((7,)),
-            dma((9,)),
-            dma((1 + 2 * classes,)),
+            dma((6,)),
+            dma((4,)),
+            dma((4,)),
+            dma((3,)),
+            dma((4,)),
+            dma((6,)),
             dma((2,)),
-            dma((2,)),
-            dma((3,)),
-            dma((3,)),
-            dma((2,)),
-            dma((2,)),
-            dma((2,)),
-            dma((2,)),
-            dma((3, n)),
-            dma((3, n)),
-            dma((classes, n)),
-            dma((classes, n)),
-            dma((classes, n)),
-            dma((classes, n)),
-            dma((2, m)),
-            dma((2, m)),
+            dma((2 + 2 * classes,)),
+            dma((1,)),
+            dma((2, m - 1)),
         ],
         compiler_params=pltpu.CompilerParams(
             collective_id=0, has_side_effects=True, vmem_limit_bytes=60 * 1024 * 1024
         ),
-    )(tokens, query_weight, key_weight, value_weight, out_weight, jnp.asarray(table), jnp.asarray(base))
+    )(tokens, query_weight, key_weight, value_weight, out_weight, jnp.asarray(table))
 
 
 def planned(n, m, *arrays):

time: 33.9 us -> 31.5 us (0.929)
  Pallas kernels: 32.9 us -> 30.6 us
    pallas_call x1, Pallas kernels: 32.9 us -> 30.6 us  [fused(): pl.pallas_call(functools.partial(fused_kernel, n, m), out_shape=pltpu.VME...]
where the time goes in v3:
time: 31.5 us; the launch traced here: 31.3 us
  Pallas kernels  30.6 us (97%)
  local copies, waits for them, and re-layouts  0.71 us (2%)
    pallas_call x1, Pallas kernels, fused(): pl.pallas_call(functools.partial(fused_kernel, n, m), out_shape=pltpu.VME...  30.6 us
    unnamed x1, local copies, waits for them, and re-layouts  0.71 us

profile of v3, /device:TPU:1, one launch (start us, length us, event | category | flops | bytes accessed | tf_op | source)
XLA Modules:
  0.0 31.3 jit_solution(4982572605706965652)
XLA Ops:
  0.0 30.6 %shard_map.64 = bf16[256,512]{1,0:T(8,128)(2,1)S(1)} custom-call(bf16[256,2048]{1,0:T(8,128)(2,1)} %tokens_hbm.1, bf16[3,2048,256]{2,1,0:T(8,128)(2,1)} %query_hbm.1, bf16[3,2048,256]{2,1,0:T(8,128)(2,1)} %key_hbm.1, bf16[3,2048,256]{2,1,0:T(8,128)(2,1)} %value_hbm.1, bf16[1024,512]{1,0:T(8,128)(2,1)} %out_hbm.1, f32[2,264,128]{2,1,0:T(8,128)} %constant.2.clone.table_hbm), custom_call_target="tpu_custom_call" | custom-call | tf_op jit(solution)/shard_map/pallas_call | solution.py:700
  30.6 0.7 %copy.8 = bf16[256,512]{1,0:T(8,128)(2,1)} copy(bf16[256,512]{1,0:T(8,128)(2,1)S(1)} %shard_map.64) | data formatting | bytes 524288

commit v4 on v3

--- a/solution.py
+++ b/solution.py
@@ -235,7 +235,7 @@
     n, m, tokens_hbm, query_hbm, key_hbm, value_hbm, out_hbm, table_hbm, result_ref,
     tokens, weights, out_weight, table, kv_first, mid_kv, mid_q, mid_send, mid_ret, mid_back,
     mid_lse, mid_lse_back, far_send, far_recv, back_send, back_recv, lse_send, lse_recv,
-    merged_all, result_wide, load_sem, weight_sem, first_sem, pair_sem, hop_sem, ret_sem,
+    merged_all, result_wide, natural, load_sem, first_sem, pair_sem, hop_sem, ret_sem,
     far_sem, back_sem, tp_send_sem, tp_recv_sem,
 ):
     me = lax.axis_index("sp")
@@ -252,6 +252,8 @@
     steps = length // MIDDLE_DILATION
     piece = length // 2
     sub = steps // 8
+    back_rows = n * (far_steps * columns // 256 + 1)
+    ret_rows = steps * columns // 256 + 8
 
     table_load = pltpu.make_async_copy(table_hbm, table, load_sem.at[0])
     table_load.start()
@@ -262,7 +264,7 @@
         sem = load_sem.at[1 + index]
         pltpu.make_async_copy(tokens_hbm.at[:, part], tokens.at[:, part], sem).start()
         pltpu.make_async_copy(key_hbm.at[2, part], weights.at[7, part], sem).start()
-    out_load = pltpu.make_async_copy(out_hbm, out_weight, load_sem.at[1 + chunks])
+    out_load = pltpu.make_async_copy(out_hbm, out_weight, load_sem.at[2])
     sources = (query_hbm, key_hbm, value_hbm)
     order = ((2, 2), (2, 0), (1, 1), (1, 2), (1, 0), (0, 1), (0, 2), (0, 0))
     waiting = []
@@ -270,7 +272,7 @@
     for index, (group, kind) in enumerate(order):
         slot = group * 3 + kind
         load = pltpu.make_async_copy(
-            sources[kind].at[group], weights.at[slot], weight_sem.at[index % 4]
+            sources[kind].at[group], weights.at[slot], load_sem.at[(5, 1, 2, 3, 4, 0, 5, 1)[index]]
         )
         weight_loads[group, kind] = load
         waiting.append(load)
@@ -287,17 +289,7 @@
             barrier, inc=1, device_id={"tp": lax.rem(mine + distance, m)}, device_id_type=MESH
         )
 
-    far_order = one_hot(
-        length, lambda row: (row % far_steps) * FAR_DILATION + row // far_steps
-    )
-    middle_order = one_hot(
-        length,
-        lambda row: (row % steps) * MIDDLE_DILATION + (row // steps + 2 * side) % MIDDLE_DILATION,
-    )
     tile = 2 * halo
-    first_order = one_hot(
-        length, lambda row: row // tile * tile + (row % halo) * 2 + row % tile // halo
-    )
     lane = lax.broadcasted_iota(jnp.int32, (1, columns), 1)
     first_half = lane % HEAD_DIM < half
 
@@ -320,7 +312,7 @@
             product = product * cosine + jnp.where(first_half, later, earlier) * sine
         if kind == 0:
             product = product * HEAD_DIM ** (-0.5)
-        return product.astype(jnp.bfloat16)
+        return product
 
     def project(group, kind):
         slot = group * 3 + kind
@@ -329,8 +321,18 @@
             waiting.pop(0).start()
         return turned(product_of(slot, 0, depth), kind)
 
-    def ordered(order, block):
-        return jnp.dot(order, block, preferred_element_type=jnp.float32).astype(jnp.bfloat16)
+    def keep(product, slot):
+        for at in range(columns // 128):
+            natural[slot, at] = product[:, at * 128 : (at + 1) * 128]
+
+    def every(slot, start, size, stride):
+        return jnp.concatenate(
+            [
+                natural[slot, at, pl.ds(start, size, stride=stride), :]
+                for at in range(columns // 128)
+            ],
+            axis=1,
+        ).astype(jnp.bfloat16)
 
     with scope("w_table"):
         table_load.wait()
@@ -354,32 +356,37 @@
 
     def far(kind):
         with scope(f"p_far{kind}"):
-            block = turned(first_product, 1) if kind == 1 else project(2, kind)
-            far_send[kind] = ordered(far_order, block).reshape(far_send.shape[1:])
+            keep(turned(first_product, 1) if kind == 1 else project(2, kind), kind)
+            for index in range(FAR_DILATION):
+                far_send[kind, index] = every(kind, index, far_steps, FAR_DILATION)
         if kind == 1:
             with scope("w_barrier"):
                 pl.semaphore_wait(barrier, n - 1 + m - 1)
+
+    def far_go(kind, index):
         for distance in range(1, n):
             target = lax.rem(me + distance, n)
             remote(
-                far_send.at[kind, pl.ds(target * classes, classes)],
-                far_recv.at[kind, :, me], far_sem.at[0], far_sem.at[1], "sp", target,
+                far_send.at[kind, target * classes + index],
+                far_recv.at[kind, index, me], far_sem.at[0], far_sem.at[1 + index], "sp", target,
             ).start()
         pltpu.make_async_copy(
-            far_send.at[kind, pl.ds(me * classes, classes)], far_recv.at[kind, :, me],
-            far_sem.at[1],
+            far_send.at[kind, me * classes + index], far_recv.at[kind, index, me],
+            far_sem.at[1 + index],
         ).start()
 
     def middle(kind):
         with scope(f"p_mid{kind}"):
-            block = ordered(middle_order, project(1, kind)).reshape(2, 2, steps, columns)
-            if kind == 0:
-                mid_q[:, pl.ds(side, 1)] = block[0][:, None]
-                landing = mid_q.at[:, side]
-            else:
-                mid_kv[kind - 1, :, pl.ds(1 + side, 1)] = block[0][:, None]
-                landing = mid_kv.at[kind - 1, :, 1 + side]
-            mid_send[kind] = block[1]
+            keep(project(1, kind), 3 + kind)
+            for index in range(2):
+                own = every(3 + kind, 2 * side + index, steps, MIDDLE_DILATION)
+                other = every(3 + kind, 2 * (1 - side) + index, steps, MIDDLE_DILATION)
+                if kind == 0:
+                    mid_q[index, pl.ds(side, 1)] = own[None]
+                else:
+                    mid_kv[kind - 1, index, pl.ds(1 + side, 1)] = own[None]
+                mid_send[kind, index] = other
+            landing = mid_q.at[:, side] if kind == 0 else mid_kv.at[kind - 1, :, 1 + side]
         remote(
             mid_send.at[kind], landing, pair_sem.at[0], pair_sem.at[1 if kind else 2],
             "sp", partner,
@@ -397,9 +404,9 @@
         hop_sem.at[2], hop_sem.at[3], "sp", lax.rem(me - 2 * lean + n, n),
     )
 
-    far(1)
-    far(2)
-    far(0)
+    for kind in (1, 2, 0):
+        far(kind)
+        far_go(kind, 0)
     middle(1)
     middle(2)
 
@@ -407,11 +414,14 @@
     def _():
         direct.start()
 
+    far_go(1, 1)
+    far_go(2, 1)
+    far_go(0, 1)
     middle(0)
 
     for kind in (1, 2):
         with scope(f"p_first{kind}"):
-            kv_first[kind - 1, halo : halo + length] = project(0, kind)
+            kv_first[kind - 1, halo : halo + length] = project(0, kind).astype(jnp.bfloat16)
 
     first_up = remote(
         kv_first.at[:, pl.ds(length, halo)], kv_first.at[:, pl.ds(0, halo)],
@@ -447,7 +457,15 @@
         mid_kv[:, :, 3] = jnp.zeros_like(mid_kv[:, :, 3])
 
     with scope("p_first0"):
-        first_queries = ordered(first_order, project(0, 0))
+        keep(project(0, 0), 6)
+        first_queries = jnp.concatenate(
+            [
+                every(6, start + part, halo, 2)
+                for start in range(0, length, tile)
+                for part in range(2)
+            ],
+            axis=0,
+        )
 
     with scope("w_pair"):
         take(mid_kv.at[:, :, 2 - side], pair_sem.at[1])
@@ -456,14 +474,15 @@
     def _():
         relay.start()
 
-    with scope("w_far"):
-        take(far_recv, far_sem.at[1])
     class_len = n * far_steps
     far_bias = band_bias(class_len, class_len, 0, 0, class_len)
     row16 = lax.broadcasted_iota(jnp.int32, (class_len, 128), 0) % far_steps
     lane16 = lax.broadcasted_iota(jnp.int32, (class_len, 128), 1)
     diagonal = lane16 % far_steps == row16
-    for index in range(classes):
+
+    def far_class(index):
+        with scope(f"w_far{index}"):
+            take(far_recv.at[:, index], far_sem.at[1 + index])
         with scope(f"c_far{index}"):
             queries, keys, values = (
                 far_recv[kind, index].reshape(class_len, columns) for kind in range(3)
@@ -476,15 +495,17 @@
             )
             lse_send[index] = jnp.sum(spread.reshape(n, far_steps, 128), axis=1, keepdims=True)
         for which, (source, landing) in enumerate(((back_send, back_recv), (lse_send, lse_recv))):
-            for distance in range(1, n):
-                target = lax.rem(me + distance, n)
+            for peer in range(n - 1):
+                target = peer + jnp.where(me <= peer, 1, 0)
                 remote(
                     source.at[index, target], landing.at[index, me],
-                    back_sem.at[which], back_sem.at[2 + 2 * index + which], "sp", target,
+                    back_sem.at[which], back_sem.at[2 + index], "sp", target,
                 ).start()
             pltpu.make_async_copy(
-                source.at[index, me], landing.at[index, me], back_sem.at[2 + 2 * index + which]
+                source.at[index, me], landing.at[index, me], back_sem.at[2 + index]
             ).start()
+
+    far_class(0)
 
     with scope("w_hop"):
         take(mid_q.at[:, 1 - side], pair_sem.at[2])
@@ -518,11 +539,13 @@
                 for head, lse in enumerate(lses)
             )
             mid_lse[index] = jnp.sum(spread.reshape(2, sub, 8, 128), axis=1)
-        for which, (source, landing) in enumerate(((mid_ret, mid_back), (mid_lse, mid_lse_back))):
+        for source, landing in ((mid_ret, mid_back), (mid_lse, mid_lse_back)):
             remote(
                 source.at[index, 1 - side], landing.at[index],
-                ret_sem.at[which], ret_sem.at[2 + 2 * index + which], "sp", partner,
+                ret_sem.at[0], ret_sem.at[1 + index], "sp", partner,
             ).start()
+
+    far_class(1)
 
     with scope("w_first"):
         @pl.when(me < n - 1)
@@ -570,11 +593,9 @@
     far_keep = (lane_part % far_steps == position) & (lane_part < heads * far_steps)
     middle_keep = (sub_lane % sub == sub_row) & (sub_lane < heads * sub)
 
-    near = []
-    for part in range(2):
+    def near(part):
         with scope(f"w_ret{part}"):
-            take(mid_back.at[part], ret_sem.at[2 + 2 * part])
-            take(mid_lse_back.at[part], ret_sem.at[3 + 2 * part])
+            take(natural.at[0, 0, pl.ds(0, ret_rows)], ret_sem.at[1 + part])
         with scope(f"c_near{part}"):
             block = jnp.concatenate([mid_ret[part, side], mid_back[part]], axis=0)
             block = jnp.dot(middle_natural, block, preferred_element_type=jnp.float32)
@@ -592,38 +613,40 @@
             top = jnp.maximum(first_lse, middle_lse)
             first_w = jnp.exp(first_lse - top)
             middle_w = jnp.exp(middle_lse - top)
-            near.append((first_w * first_out + middle_w * block, first_w + middle_w, top))
+        return first_w * first_out + middle_w * block, first_w + middle_w, top
 
     chips = m // 2
     sibling = mine + 1 - 2 * lax.rem(mine, 2)
 
+    core = lax.rem(mine, 2)
+
+    def rows_of(part):
+        return pl.ds(part * piece, piece)
+
     def hand(part, source, slot, target):
-        rows = pl.ds(part * piece, piece)
-        copy = remote(
-            merged_all.at[source, rows], merged_all.at[slot, rows],
+        remote(
+            merged_all.at[source, rows_of(part)], merged_all.at[slot, rows_of(part)],
             tp_send_sem.at[0], tp_recv_sem.at[part, slot - 1], "tp", target,
-        )
-        copy.start()
-        return copy
-
-    def term(part, slot):
-        chip = slot % chips
-        owner = lax.rem((mine if slot < chips else sibling) - 2 * chip + m, m)
-        rows = pl.ds(pl.multiple_of(owner * columns, columns), columns)
+        ).start()
+
+    def arrived(part, slot):
+        take(merged_all.at[slot, rows_of(part)], tp_recv_sem.at[part, slot - 1])
+
+    def term(part, slot, owner):
+        rows = pl.ds(pl.multiple_of(lax.rem(owner + m, m) * columns, columns), columns)
         return jnp.dot(
             merged_all[slot, part * piece : (part + 1) * piece],
             out_weight[rows, :],
             preferred_element_type=jnp.float32,
         )
 
-    copies = {}
     totals = []
     with scope("w_outw"):
         out_load.wait()
     for part in range(2):
+        total, weight, near_top = near(part)
         with scope(f"w_back{part}"):
-            take(back_recv.at[part], back_sem.at[2 + 2 * part])
-            take(lse_recv.at[part], back_sem.at[3 + 2 * part])
+            take(natural.at[0, 0, pl.ds(0, back_rows)], back_sem.at[2 + part])
         with scope(f"c_merge{part}"):
             far_out = jnp.dot(
                 far_natural,
@@ -633,47 +656,67 @@
             lse = jnp.concatenate([lse_recv[part].reshape(n, 128)] * (piece // n), axis=0)
             lse = jnp.where(far_keep, lse, 0.0)
             far_lse = jnp.dot(in_terms(lse), far_spread, preferred_element_type=jnp.float32)
-            total, weight, near_top = near[part]
             top = jnp.maximum(near_top, far_lse)
             near_w = jnp.exp(near_top - top)
             far_w = jnp.exp(far_lse - top)
             merged = (near_w * total + far_w * far_out) / (near_w * weight + far_w)
             merged_all[0, part * piece : (part + 1) * piece] = merged.astype(jnp.bfloat16)
         for chip in range(1, chips):
-            copies[part, chip] = hand(part, 0, chip, lax.rem(mine + 2 * chip, m))
-        copies[part, chips] = hand(part, 0, chips, sibling)
-        totals.append(term(part, 0))
+            hand(part, 0, chip, lax.rem(mine + 2 * chip, m))
+            if part == 1:
+                @pl.when(core == 0)
+                def _():
+                    hand(part, 0, chips + chip, lax.rem(mine + 2 * chip + 1, m))
+        hand(part, 0, chips, sibling)
+        totals.append(term(part, 0, mine))
 
     take(mid_send, pair_sem.at[0])
     take(far_send.at[:, pl.ds(0, FAR_DILATION - classes)], far_sem.at[0])
     take(back_send.at[:, pl.ds(0, n - 1)], back_sem.at[0])
     take(lse_send.at[:, pl.ds(0, n - 1)], back_sem.at[1])
-    take(mid_back, ret_sem.at[0])
-    take(mid_lse_back, ret_sem.at[1])
-
-    for part in range(2):
-        for chip in range(1, chips):
-            with scope(f"w_chip{part}"):
-                copies[part, chip].wait_recv()
-            copies[part, chips + chip] = hand(part, chip, chips + chip, sibling)
-        with scope(f"w_sib{part}"):
-            copies[part, chips].wait_recv()
-        totals[part] = totals[part] + term(part, chips)
-        for chip in range(1, chips):
-            totals[part] = totals[part] + term(part, chip)
-    for part in range(2):
-        for chip in range(1, chips):
-            with scope(f"w_fwd{part}"):
-                copies[part, chips + chip].wait_recv()
-            totals[part] = totals[part] + term(part, chips + chip)
+    take(natural.at[0, 0, pl.ds(0, 2 * ret_rows)], ret_sem.at[0])
+
+    for chip in range(1, chips):
+        with scope("w_chip0"):
+            arrived(0, chip)
+        hand(0, chip, chips + chip, sibling)
+    with scope("w_sib0"):
+        arrived(0, chips)
+    totals[0] = totals[0] + term(0, chips, sibling)
+    for chip in range(1, chips):
+        totals[0] = totals[0] + term(0, chip, mine - 2 * chip)
+    for chip in range(1, chips):
+        early = jnp.where(core == 1, chip, chips + chip)
+        with scope("w_early"):
+            arrived(1, early)
+
+        @pl.when(core == 1)
+        def _():
+            hand(1, chip, chips + chip, sibling)
+
+        totals[1] = totals[1] + term(1, early, mine + 1 - core - 2 * chip)
+    with scope("w_sib1"):
+        arrived(1, chips)
+    totals[1] = totals[1] + term(1, chips, sibling)
+    for chip in range(1, chips):
+        with scope("w_fwd0"):
+            arrived(0, chips + chip)
+        totals[0] = totals[0] + term(0, chips + chip, sibling - 2 * chip)
+    for chip in range(1, chips):
+        late = jnp.where(core == 1, chips + chip, chip)
+        with scope("w_late"):
+            arrived(1, late)
+        totals[1] = totals[1] + term(1, late, mine - core - 2 * chip)
+    with scope("c_result"):
+        for part in range(2):
+            for index in range(result_wide.shape[0]):
+                result_wide[index, pl.ds(part, piece, stride=2), :] = totals[part][
+                    :, index * 128 : (index + 1) * 128
+                ]
         for index in range(result_wide.shape[0]):
-            result_wide[index, pl.ds(part, piece, stride=2), :] = totals[part][
-                :, index * 128 : (index + 1) * 128
-            ]
-    for index in range(result_wide.shape[0]):
-        result_ref[:, index * 128 : (index + 1) * 128] = result_wide[index].astype(
-            result_ref.dtype
-        )
+            result_ref[:, index * 128 : (index + 1) * 128] = result_wide[index].astype(
+                result_ref.dtype
+            )
     take(merged_all.at[pl.ds(1, m - 1)], tp_send_sem.at[0])
 
 
@@ -723,14 +766,14 @@
             pltpu.VMEM((classes, n, 1, 128), jnp.float32),
             pltpu.VMEM((m, length, columns), bf16),
             pltpu.VMEM((out_weight.shape[1] // 128, length, 128), jnp.float32),
+            pltpu.VMEM((7, columns // 128, length, 128), jnp.float32),
             dma((6,)),
-            dma((4,)),
             dma((4,)),
             dma((3,)),
             dma((4,)),
-            dma((6,)),
-            dma((2,)),
-            dma((2 + 2 * classes,)),
+            dma((3,)),
+            dma((1 + classes,)),
+            dma((2 + classes,)),
             dma((1,)),
             dma((2, m - 1)),
         ],

time: 31.5 us -> 30.3 us (0.962)
  Pallas kernels: 30.6 us -> 29.5 us
    pallas_call x1, Pallas kernels: 30.6 us -> 29.5 us  [fused(): pl.pallas_call(functools.partial(fused_kernel, n, m), out_shape=pltpu.VME...]
where the time goes in v4:
time: 30.3 us; the launch traced here: 30.2 us
  Pallas kernels  29.5 us (97%)
  local copies, waits for them, and re-layouts  0.71 us (2%)
    pallas_call x1, Pallas kernels, fused(): pl.pallas_call(functools.partial(fused_kernel, n, m), out_shape=pltpu.VME...  29.5 us
    unnamed x1, local copies, waits for them, and re-layouts  0.71 us

profile of v4, /device:TPU:1, one launch (start us, length us, event | category | flops | bytes accessed | tf_op | source)
XLA Modules:
  0.0 30.2 jit_solution(5541596887750533301)
XLA Ops:
  0.0 29.5 %shard_map.64 = bf16[256,512]{1,0:T(8,128)(2,1)S(1)} custom-call(bf16[256,2048]{1,0:T(8,128)(2,1)} %tokens_hbm.1, bf16[3,2048,256]{2,1,0:T(8,128)(2,1)} %query_hbm.1, bf16[3,2048,256]{2,1,0:T(8,128)(2,1)} %key_hbm.1, bf16[3,2048,256]{2,1,0:T(8,128)(2,1)} %value_hbm.1, bf16[1024,512]{1,0:T(8,128)(2,1)} %out_hbm.1, f32[2,264,128]{2,1,0:T(8,128)} %constant.2.clone.table_hbm), custom_call_target="tpu_custom_call" | custom-call | tf_op jit(solution)/shard_map/pallas_call | solution.py:743
  29.5 0.7 %copy.8 = bf16[256,512]{1,0:T(8,128)(2,1)} copy(bf16[256,512]{1,0:T(8,128)(2,1)S(1)} %shard_map.64) | data formatting | bytes 524288

commit v5 on v4

--- a/solution.py
+++ b/solution.py
@@ -256,7 +256,6 @@
     ret_rows = steps * columns // 256 + 8
 
     table_load = pltpu.make_async_copy(table_hbm, table, load_sem.at[0])
-    table_load.start()
     chunks = 4
     chunk = depth // chunks
     for index in range(chunks):
@@ -264,9 +263,11 @@
         sem = load_sem.at[1 + index]
         pltpu.make_async_copy(tokens_hbm.at[:, part], tokens.at[:, part], sem).start()
         pltpu.make_async_copy(key_hbm.at[2, part], weights.at[7, part], sem).start()
+        if index == 1:
+            table_load.start()
     out_load = pltpu.make_async_copy(out_hbm, out_weight, load_sem.at[2])
     sources = (query_hbm, key_hbm, value_hbm)
-    order = ((2, 2), (2, 0), (1, 1), (1, 2), (1, 0), (0, 1), (0, 2), (0, 0))
+    order = ((2, 2), (1, 1), (1, 2), (2, 0), (1, 0), (0, 1), (0, 2), (0, 0))
     waiting = []
     weight_loads = {}
     for index, (group, kind) in enumerate(order):
@@ -334,6 +335,12 @@
             axis=1,
         ).astype(jnp.bfloat16)
 
+    first_product = None
+    for index in range(chunks):
+        with scope(f"w_load{index}"):
+            take(weights.at[7, pl.ds(0, 2 * chunk)], load_sem.at[1 + index])
+        term = product_of(7, index * chunk, chunk)
+        first_product = term if first_product is None else first_product + term
     with scope("w_table"):
         table_load.wait()
     base_cos = table[0, pl.ds(length + me, 1), :]
@@ -345,20 +352,17 @@
     wide = columns // cosine.shape[1]
     cosine = jnp.concatenate([cosine] * wide, axis=1)
     sine = jnp.concatenate([sine] * wide, axis=1) * jnp.where(first_half, -1.0, 1.0)
-    first_product = None
-    for index in range(chunks):
-        with scope(f"w_load{index}"):
-            take(weights.at[7, pl.ds(0, 2 * chunk)], load_sem.at[1 + index])
-        term = product_of(7, index * chunk, chunk)
-        first_product = term if first_product is None else first_product + term
     for _ in range(3):
         waiting.pop(0).start()
+
+    def far_pick(kind, parity):
+        for index in range(parity, FAR_DILATION, classes):
+            far_send[kind, index] = every(kind, index, far_steps, FAR_DILATION)
 
     def far(kind):
         with scope(f"p_far{kind}"):
             keep(turned(first_product, 1) if kind == 1 else project(2, kind), kind)
-            for index in range(FAR_DILATION):
-                far_send[kind, index] = every(kind, index, far_steps, FAR_DILATION)
+            far_pick(kind, 0)
         if kind == 1:
             with scope("w_barrier"):
                 pl.semaphore_wait(barrier, n - 1 + m - 1)
@@ -404,9 +408,10 @@
         hop_sem.at[2], hop_sem.at[3], "sp", lax.rem(me - 2 * lean + n, n),
     )
 
-    for kind in (1, 2, 0):
-        far(kind)
-        far_go(kind, 0)
+    far(1)
+    far_go(1, 0)
+    far(2)
+    far_go(2, 0)
     middle(1)
     middle(2)
 
@@ -414,9 +419,11 @@
     def _():
         direct.start()
 
-    far_go(1, 1)
-    far_go(2, 1)
-    far_go(0, 1)
+    far(0)
+    far_go(0, 0)
+    for kind in (1, 2, 0):
+        far_pick(kind, 1)
+        far_go(kind, 1)
     middle(0)
 
     for kind in (1, 2):
@@ -525,7 +532,7 @@
     middle_bias = band_bias(2 * steps, 4 * steps, -steps, low, high)
     sub_row = lax.broadcasted_iota(jnp.int32, (2 * steps, 128), 0) % steps // 8
     sub_lane = lax.broadcasted_iota(jnp.int32, (2 * steps, 128), 1)
-    for index in range(2):
+    def middle_class(index):
         with scope(f"c_mid{index}"):
             out, lses = attend(
                 mid_q[index].reshape(2 * steps, columns),
@@ -545,7 +552,9 @@
                 ret_sem.at[0], ret_sem.at[1 + index], "sp", partner,
             ).start()
 
+    middle_class(0)
     far_class(1)
+    middle_class(1)
 
     with scope("w_first"):
         @pl.when(me < n - 1)
@@ -661,13 +670,13 @@
             far_w = jnp.exp(far_lse - top)
             merged = (near_w * total + far_w * far_out) / (near_w * weight + far_w)
             merged_all[0, part * piece : (part + 1) * piece] = merged.astype(jnp.bfloat16)
+        hand(part, 0, chips, sibling)
         for chip in range(1, chips):
             hand(part, 0, chip, lax.rem(mine + 2 * chip, m))
             if part == 1:
                 @pl.when(core == 0)
                 def _():
                     hand(part, 0, chips + chip, lax.rem(mine + 2 * chip + 1, m))
-        hand(part, 0, chips, sibling)
         totals.append(term(part, 0, mine))
 
     take(mid_send, pair_sem.at[0])

time: 30.3 us -> 29.8 us (0.983)
  Pallas kernels: 29.5 us -> 28.9 us
    pallas_call x1, Pallas kernels: 29.5 us -> 28.9 us  [fused(): pl.pallas_call(functools.partial(fused_kernel, n, m), out_shape=pltpu.VME...]
where the time goes in v5:
time: 29.8 us; the launch traced here: 29.7 us
  Pallas kernels  28.9 us (97%)
  local copies, waits for them, and re-layouts  0.71 us (2%)
    pallas_call x1, Pallas kernels, fused(): pl.pallas_call(functools.partial(fused_kernel, n, m), out_shape=pltpu.VME...  28.9 us
    unnamed x1, local copies, waits for them, and re-layouts  0.71 us

profile of v5, /device:TPU:1, one launch (start us, length us, event | category | flops | bytes accessed | tf_op | source)
XLA Modules:
  0.0 29.7 jit_solution(1535279711876353668)
XLA Ops:
  0.0 28.9 %shard_map.64 = bf16[256,512]{1,0:T(8,128)(2,1)S(1)} custom-call(bf16[256,2048]{1,0:T(8,128)(2,1)} %tokens_hbm.1, bf16[3,2048,256]{2,1,0:T(8,128)(2,1)} %query_hbm.1, bf16[3,2048,256]{2,1,0:T(8,128)(2,1)} %key_hbm.1, bf16[3,2048,256]{2,1,0:T(8,128)(2,1)} %value_hbm.1, bf16[1024,512]{1,0:T(8,128)(2,1)} %out_hbm.1, f32[2,264,128]{2,1,0:T(8,128)} %constant.2.clone.table_hbm), custom_call_target="tpu_custom_call" | custom-call | tf_op jit(solution)/shard_map/pallas_call | solution.py:752
  29.0 0.7 %copy.8 = bf16[256,512]{1,0:T(8,128)(2,1)} copy(bf16[256,512]{1,0:T(8,128)(2,1)S(1)} %shard_map.64) | data formatting | bytes 524288

commit v6 on v5

--- a/solution.py
+++ b/solution.py
@@ -412,6 +412,13 @@
     far_go(1, 0)
     far(2)
     far_go(2, 0)
+
+    @pl.when(me >= n // 2)
+    def _():
+        for kind in (1, 2):
+            far_pick(kind, 1)
+            far_go(kind, 1)
+
     middle(1)
     middle(2)
 
@@ -421,9 +428,14 @@
 
     far(0)
     far_go(0, 0)
-    for kind in (1, 2, 0):
-        far_pick(kind, 1)
-        far_go(kind, 1)
+    @pl.when(me < n // 2)
+    def _():
+        for kind in (1, 2):
+            far_pick(kind, 1)
+            far_go(kind, 1)
+
+    far_pick(0, 1)
+    far_go(0, 1)
     middle(0)
 
     for kind in (1, 2):
@@ -513,6 +525,10 @@
             ).start()
 
     far_class(0)
+
+    @pl.when(me >= 2)
+    def _():
+        far_class(1)
 
     with scope("w_hop"):
         take(mid_q.at[:, 1 - side], pair_sem.at[2])
@@ -553,8 +569,12 @@
             ).start()
 
     middle_class(0)
-    far_class(1)
     middle_class(1)
+
+    @pl.when(me < 2)
+    def _():
+        far_class(1)
+
 
     with scope("w_first"):
         @pl.when(me < n - 1)

time: 29.8 us -> 29.7 us (level)
  no operation moved by 1% of the time
where the time goes in v6:
time: 29.7 us; the launch traced here: 29.5 us
  Pallas kernels  28.8 us (97%)
  local copies, waits for them, and re-layouts  0.71 us (2%)
    pallas_call x1, Pallas kernels, fused(): pl.pallas_call(functools.partial(fused_kernel, n, m), out_shape=pltpu.VME...  28.8 us
    unnamed x1, local copies, waits for them, and re-layouts  0.71 us

profile of v6, /device:TPU:1, one launch (start us, length us, event | category | flops | bytes accessed | tf_op | source)
XLA Modules:
  0.0 29.5 jit_solution(3769874626274137022)
XLA Ops:
  0.0 28.8 %shard_map.64 = bf16[256,512]{1,0:T(8,128)(2,1)S(1)} custom-call(bf16[256,2048]{1,0:T(8,128)(2,1)} %tokens_hbm.1, bf16[3,2048,256]{2,1,0:T(8,128)(2,1)} %query_hbm.1, bf16[3,2048,256]{2,1,0:T(8,128)(2,1)} %key_hbm.1, bf16[3,2048,256]{2,1,0:T(8,128)(2,1)} %value_hbm.1, bf16[1024,512]{1,0:T(8,128)(2,1)} %out_hbm.1, f32[2,264,128]{2,1,0:T(8,128)} %constant.2.clone.table_hbm), custom_call_target="tpu_custom_call" | custom-call | tf_op jit(solution)/shard_map/pallas_call | solution.py:772
  28.8 0.7 %copy.8 = bf16[256,512]{1,0:T(8,128)(2,1)} copy(bf16[256,512]{1,0:T(8,128)(2,1)S(1)} %shard_map.64) | data formatting | bytes 524288
